TPU v7x, 32 devices: a whole 2x2x4 slice. The times are simulated.
32 devices in a mesh: sp: 16 (over z, y, core), tp: 2 (over x).
Axes of the slice: x: 2, y: 2, z: 4, core: 2. Of those that a mesh axis runs over, the one named last changes fastest.
Arguments:
- query_rows: bfloat16 [10240, 1536], P('sp', 'tp'), may hold values from -8 to 8
- key_rows: bfloat16 [10240, 1536], P('sp', 'tp'), may hold values from -8 to 8
- value_rows: bfloat16 [10240, 1536], P('sp', 'tp'), may hold values from -6 to 6
- query_gain: bfloat16 [64], replicated, may hold values from 0.25 to 4.2
- key_gain: bfloat16 [64], replicated, may hold values from 0.25 to 4.2
- position_bias: bfloat16 [24, 320], P('tp'), may hold values from -165 to 3
- output_grad: bfloat16 [10240, 1536], P('sp', 'tp'), may hold values from -24 to 24
Outputs:
- query_grad: bfloat16 [10240, 1536], P('sp', 'tp')
- key_grad: bfloat16 [10240, 1536], P('sp', 'tp')
- value_grad: bfloat16 [10240, 1536], P('sp', 'tp')
- bias_grad: float32 [24, 320], P('tp')
- query_gain_grad: float32 [64], replicated
- key_gain_grad: float32 [64], replicated
All inputs are finite; a program needn't handle non-finite values.
Results may differ from a plain program's by a relative error of at most 0.0055.
The roundings to bfloat16 on the way count: a program that leaves them out, or rounds other values in their place, can miss the bound.
Values may be sent and summed in bfloat16 or wider, within the bound.
A program may use at most 128 MiB of HBM per device.

v0:
```python
import jax
import jax.numpy as jnp
import numpy as np
from jax import lax
from jax.sharding import PartitionSpec as P

SEG = 64
LEFT = 8
BAND = 576
RSPAN = 320


NORM_EPS = 1e-06


def passed_along(block, axis, distance):
    devices = range(lax.axis_size(axis))
    route = [(i - distance, i) for i in devices if i - distance in devices]
    return lax.ppermute(block, axis, route)


def unit_rows(values):
    widened = values.astype(jnp.float32)
    scale_rows = lax.rsqrt(jnp.mean(widened * widened, axis=-1, keepdims=True) + NORM_EPS)
    return (widened * scale_rows, scale_rows)


def band_of(segments, seg_count):
    return jnp.concatenate(
        [segments[offset : offset + seg_count] for offset in range(LEFT + 1)], axis=1
    )


def unband(banded, seg_count):
    summed = jnp.zeros((seg_count + LEFT, SEG) + banded.shape[2:], jnp.float32)
    for offset in range(LEFT + 1):
        summed = summed.at[offset : offset + seg_count].add(
            banded[:, offset * SEG : (offset + 1) * SEG]
        )
    return summed


def head_major(matrix, head_count):
    return matrix.reshape(matrix.shape[0], head_count, -1).transpose(1, 0, 2)


def row_major(stacked):
    return stacked.transpose(1, 0, 2).reshape(stacked.shape[1], -1)


def bias_matrix_of(bias_table):
    head_count = bias_table.shape[0]
    extent = BAND + SEG - 1
    tail_fill = jnp.broadcast_to(bias_table[:, -1:], (head_count, extent - bias_table.shape[1]))
    extended = jnp.concatenate([bias_table, tail_fill], axis=1)
    shifted = jnp.roll(extended[:, ::-1], -(SEG - 1), axis=1)
    tiled = jnp.tile(shifted, (1, SEG))[:, : SEG * (extent - 1)]
    return tiled.reshape(head_count, SEG, extent - 1)[:, :, :BAND]


def bias_grad_of(summed):
    head_count = summed.shape[0]
    extent = BAND + SEG - 1
    padded = jnp.pad(summed[:, ::-1, :], ((0, 0), (0, 0), (0, SEG)))
    skewed = padded.reshape(head_count, SEG * (extent + 1))[:, : SEG * extent].reshape(
        head_count, SEG, extent
    )
    by_distance = jnp.sum(skewed, axis=1)[:, ::-1]
    return jnp.concatenate(
        [by_distance[:, : RSPAN - 1], jnp.sum(by_distance[:, RSPAN - 1 :], axis=1, keepdims=True)],
        axis=1,
    )


def backward_block(query_seg, grad_seg, key_band, value_band, row_bias, visible):
    score_scale = query_seg.shape[-1] ** (-0.5)
    scores = (
        jnp.einsum("cqd,ckd->cqk", query_seg, key_band, preferred_element_type=jnp.float32)
        * score_scale
        + row_bias[None]
    )
    scores = jnp.where(visible[:, None, :], scores, -jnp.inf)
    d_weights = jnp.einsum("cqd,ckd->cqk", grad_seg, value_band, preferred_element_type=jnp.float32)
    row_peak = jnp.max(scores, axis=-1)
    raised = jnp.exp(scores - row_peak[..., None])
    row_total = jnp.sum(raised, axis=-1)
    weights = raised / row_total[..., None]
    row_delta = jnp.sum(weights * d_weights, axis=-1)
    d_scores = weights * (d_weights - row_delta[..., None])
    weights_low = weights.astype(jnp.bfloat16)
    d_low = d_scores.astype(jnp.bfloat16)
    dq_unit = (
        jnp.einsum("cqk,ckd->cqd", d_low, key_band, preferred_element_type=jnp.float32)
        * score_scale
    )
    dk_band = (
        jnp.einsum("cqk,cqd->ckd", d_low, query_seg, preferred_element_type=jnp.float32)
        * score_scale
    )
    dv_band = jnp.einsum("cqk,cqd->ckd", weights_low, grad_seg, preferred_element_type=jnp.float32)
    return (dq_unit, dk_band, dv_band, d_scores, (row_peak, row_total, row_delta))


def body(query_rows, key_rows, value_rows, query_gain, key_gain, position_bias, output_grad):
    head_count = position_bias.shape[0]
    tokens = query_rows.shape[0]
    head_size = query_gain.shape[0]
    seg_count = tokens // SEG
    reach_rows = LEFT * SEG
    gain_query = query_gain.astype(jnp.float32)
    gain_key = key_gain.astype(jnp.float32)
    query_hat, query_scale = unit_rows(head_major(query_rows, head_count))
    key_hat, key_scale = unit_rows(head_major(key_rows, head_count))
    query_unit = (query_hat * gain_query).astype(jnp.bfloat16)
    key_unit = (key_hat * gain_key).astype(jnp.bfloat16)
    value_heads = head_major(value_rows, head_count)
    cotangent_heads = head_major(output_grad, head_count)
    bias_mats = bias_matrix_of(position_bias.astype(jnp.float32))
    band_pos = np.repeat(np.arange(LEFT + 1), SEG)
    first_seg = lax.axis_index("sp") * seg_count
    visible = first_seg + jnp.arange(seg_count)[:, None] - LEFT + band_pos[None, :] >= 0
    prior_key, prior_value = passed_along(
        (
            key_unit[:, tokens - reach_rows :].reshape(head_count, reach_rows * head_size),
            value_heads[:, tokens - reach_rows :].reshape(head_count, reach_rows * head_size),
        ),
        "sp",
        1,
    )
    key_ext = jnp.concatenate(
        [prior_key.reshape(head_count, reach_rows, head_size), key_unit], axis=1
    )
    key_ext = key_ext.reshape(head_count, seg_count + LEFT, SEG, head_size)
    value_ext = jnp.concatenate(
        [prior_value.reshape(head_count, reach_rows, head_size), value_heads], axis=1
    )
    value_ext = value_ext.reshape(head_count, seg_count + LEFT, SEG, head_size)

    def main_head(inputs):
        query_head, grad_head, key_segs, value_segs, row_bias = inputs
        outputs = backward_block(
            query_head.reshape(seg_count, SEG, head_size),
            grad_head.reshape(seg_count, SEG, head_size),
            band_of(key_segs, seg_count),
            band_of(value_segs, seg_count),
            row_bias,
            visible,
        )
        return (
            outputs[0].reshape(tokens, head_size),
            unband(outputs[1], seg_count),
            unband(outputs[2], seg_count),
            jnp.sum(outputs[3], axis=0),
            outputs[4],
        )

    dq_unit, dk_ext, dv_ext, score_sums, row_stats = lax.map(
        main_head, (query_unit, cotangent_heads, key_ext, value_ext, bias_mats)
    )
    dk_unit = dk_ext[:, LEFT:].reshape(head_count, tokens, head_size)
    dv_own = dv_ext[:, LEFT:].reshape(head_count, tokens, head_size)
    back_key, back_value = passed_along(
        (
            dk_ext[:, :LEFT].reshape(head_count, reach_rows * head_size).astype(jnp.bfloat16),
            dv_ext[:, :LEFT].reshape(head_count, reach_rows * head_size).astype(jnp.bfloat16),
        ),
        "sp",
        -1,
    )
    from_later_key = back_key.reshape(head_count, reach_rows, head_size).astype(jnp.float32)
    from_later_value = back_value.reshape(head_count, reach_rows, head_size).astype(jnp.float32)
    front_pad = ((0, 0), (tokens - reach_rows, 0), (0, 0))
    dk_unit = dk_unit + jnp.pad(from_later_key, front_pad)
    value_grad = dv_own + jnp.pad(from_later_value, front_pad)
    bias_part = bias_grad_of(score_sums)
    query_gain_part = jnp.sum(dq_unit * query_hat, axis=(0, 1))
    key_gain_part = jnp.sum(dk_unit * key_hat, axis=(0, 1))
    zero_index = jnp.zeros((), jnp.int32)
    head_start = lax.axis_index("tp") * head_count
    full_table = jnp.zeros((head_count * lax.axis_size("tp"), bias_part.shape[1]), jnp.float32)
    full_table = lax.dynamic_update_slice(full_table, bias_part, (head_start, zero_index))
    full_table, query_gain_grad, key_gain_grad = lax.psum(
        (full_table, query_gain_part, key_gain_part), ("sp", "tp")
    )
    bias_grad = lax.dynamic_slice(
        full_table, (head_start, zero_index), (head_count, bias_part.shape[1])
    )
    dq_scaled = dq_unit * gain_query
    query_grad = query_scale * (
        dq_scaled - query_hat * jnp.mean(dq_scaled * query_hat, axis=-1, keepdims=True)
    )
    dk_scaled = dk_unit * gain_key
    key_grad = key_scale * (
        dk_scaled - key_hat * jnp.mean(dk_scaled * key_hat, axis=-1, keepdims=True)
    )
    return (
        row_major(query_grad.astype(jnp.bfloat16)),
        row_major(key_grad.astype(jnp.bfloat16)),
        row_major(value_grad.astype(jnp.bfloat16)),
        bias_grad,
        query_gain_grad,
        key_gain_grad,
    )


def solution(mesh):
    placed = (P("sp", "tp"), P("sp", "tp"), P("sp", "tp"), P(), P(), P("tp", None), P("sp", "tp"))
    return jax.shard_map(
        body,
        mesh=mesh,
        in_specs=placed,
        out_specs=(P("sp", "tp"), P("sp", "tp"), P("sp", "tp"), P("tp", None), P(), P()),
        check_vma=False,
    )
```

profile of v0, /device:TPU:0, one launch (start us, length us, event | category | flops | bytes accessed | tf_op | source)
XLA Modules:
  0.0 525.3 jit_solution(7589541615684947852)
XLA Ops:
  13.8 3.7 reshape.769
  17.5 4.8 collective-permute-start.1
  26.5 3.9 tile.10
  33.8 4.3 reshape.766
  41.9 3.5 reshape.764
  50.4 6.5 %reshape.765 = bf16[12,18,64,64]{2,1,3,0:T(8,128)(2,1)} reshape(bf16[12,1152,64]{1,2,0:T(8,128)(2,1)} %pad_maximum_fusion) | data formatting | bytes 3538944 | tf_op jit(solution)/shard_map/reshape | solution.py:133
  56.9 5.2 copy.31
  68.6 6.5 %reshape.771 = bf16[12,18,64,64]{2,1,3,0:T(8,128)(2,1)} reshape(bf16[12,1152,64]{1,2,0:T(8,128)(2,1)} %pad_maximum_fusion.1) | data formatting | bytes 3538944 | tf_op jit(solution)/shard_map/reshape | solution.py:137
  75.1 5.2 copy.33
  80.3 324.4 %while.38 = (s32[]{:T(128)}, f32[12,640,64]{1,2,0:T(8,128)}, f32[12,18,64,64]{2,3,1,0:T(8,128)}, f32[12,18,64,64]{2,3,1,0:T(8,128)}, f32[12,64,576]{2,1,0:T(8,12...) while((s32[]{:T(128)}, f32[12,640,64]{1,2,0:T(8,128)}, ...), condition=%wide.region_7.8_spmd.clone, body=%wide.region_2.7_spmd.clone.sunk | while | flops 242498752 | bytes 46021568 | solution.py:157
  80.9 4.2 dynamic-slice_bitcast_fusion.21
  107.9 4.4 dynamic-slice_bitcast_fusion.21
  135.2 3.9 dynamic-slice_bitcast_fusion.21
  162.1 4.0 dynamic-slice_bitcast_fusion.21
  189.1 4.3 dynamic-slice_bitcast_fusion.21
  216.2 4.1 dynamic-slice_bitcast_fusion.21
  243.2 4.1 dynamic-slice_bitcast_fusion.21
  270.2 3.8 dynamic-slice_bitcast_fusion.21
  296.9 3.9 dynamic-slice_bitcast_fusion.21
  323.7 4.3 dynamic-slice_bitcast_fusion.21
  350.8 4.0 dynamic-slice_bitcast_fusion.21
  377.8 4.1 dynamic-slice_bitcast_fusion.21
  413.6 4.5 slice.848
  428.4 4.6 slice.850
  435.3 5.5 %copy.35 = f32[12,10,64,64]{3,2,1,0:T(8,128)} copy(f32[12,10,64,64]{2,3,1,0:T(8,128)} %slice.848) | data formatting | bytes 3932160 | tf_op jit(solution)/shard_map/slice | solution.py:160
  440.8 3.7 copy.38
  445.2 5.5 %copy.39 = f32[12,10,64,64]{3,2,1,0:T(8,128)} copy(f32[12,10,64,64]{2,3,1,0:T(8,128)} %slice.850) | data formatting | bytes 3932160 | tf_op jit(solution)/shard_map/slice | solution.py:161
  452.4 3.6 convert_element_type.92
  457.9 3.5 convert_element_type.90
  463.1 3.6 fusion.41
  473.8 41.8 %all-reduce.5 = (f32[24,320]{1,0:T(8,128)S(1)}, f32[64]{0:T(128)}, f32[64]{0:T(128)}) all-reduce(f32[24,320]{1,0:T(8,128)S(1)} %dynamic_update_slice.34, f32[64]{0:T(128)S(1)} %get-tuple-element.540, f32[64]{0:T(128)S(1)} %get-tuple-element.473), channel_id=1, replica_groups=mesh['sp'=16,'tp'=2] {'sp','tp'}, use_global_device_ids=true, to_apply=%region_12.13 | all-reduce | flops 7808 | bytes 62464 | tf_op jit(solution)/shard_map/psum | solution.py:182
  516.3 3.4 convert_element_type.93
  (638 shorter events, 348.3 us)
Async XLA Ops:
  0.6 1.9 copy-start.16
  7.2 34.7 %collective-permute-start = (bf16[12,32768]{1,0:T(8,128)(2,1)}, bf16[12,32768]{1,0:T(8,128)(2,1)}, u32[]{:S(2)}, u32[]{:S(2)}) collective-permute-start(bf16[12,32768]{1,0:T(8,128)(2,1)} %reshape.763), channel_id=1, source_target_pairs={{0,2},{2,4},{4,6},{6,8},{8,10},{10,12},{12,14},{14,16},{16,18},{18... | collective-permute-start | bytes 2359304 | tf_op jit(solution)/shard_map/ppermute | solution.py:19
  12.2 10.0 %copy-start.13 = (bf16[12,320]{1,0:T(8,128)(2,1)S(1)}, bf16[12,320]{1,0:T(8,128)(2,1)}, u32[]{:S(2)}) copy-start(bf16[12,320]{1,0:T(8,128)(2,1)} %param.51) | copy-start | bytes 23044
  13.8 11.1 %copy-start.17 = (bf16[64]{0:T(256)(128)(2,1)S(1)}, bf16[64]{0:T(256)(128)(2,1)}, u32[]{:S(2)}) copy-start(bf16[64]{0:T(256)(128)(2,1)} %param.49) | copy-start | bytes 388
  17.5 44.6 %collective-permute-start.1 = (bf16[12,32768]{1,0:T(8,128)(2,1)}, bf16[12,32768]{1,0:T(8,128)(2,1)}, u32[]{:S(2)}, u32[]{:S(2)}) collective-permute-start(bf16[12,32768]{1,0:T(8,128)(2,1)} %reshape.769), channel_id=1, source_target_pairs={{0,2},{2,4},{4,6},{6,8},{8,10},{10,12},{12,14},{14,16},{16,18},{18... | collective-permute-start | bytes 2359304 | tf_op jit(solution)/shard_map/ppermute | solution.py:19
  24.9 15.7 %copy-start = (bf16[640,768]{0,1:T(8,128)(2,1)}, bf16[640,768]{0,1:T(8,128)(2,1)S(1)}, u32[]{:S(2)}) copy-start(bf16[640,768]{0,1:T(8,128)(2,1)S(1)} %copy.22) | copy-start | bytes 2949124
  24.9 15.7 %copy-start.14 = (f32[64]{0:T(128)}, f32[64]{0:T(128)S(1)}, u32[]{:S(2)}) copy-start(f32[64]{0:T(128)S(1)} %convert_element_type.80) | copy-start | bytes 772
  40.6 1.3 copy-start.9
  41.9 5.9 %copy-start.6 = (bf16[12,640,64]{1,2,0:T(8,128)(2,1)S(1)}, bf16[12,640,64]{1,2,0:T(8,128)(2,1)}, u32[]{:S(2)}) copy-start(bf16[12,640,64]{1,2,0:T(8,128)(2,1)} %copy-done.5) | copy-start | bytes 2949124
  75.1 5.2 copy-start.12
  102.3 1.2 copy-start.4
  105.1 2.1 copy-start.3
  132.4 2.1 copy-start.3
  159.3 2.1 copy-start.3
  186.3 2.1 copy-start.3
  213.4 2.1 copy-start.3
  240.4 2.1 copy-start.3
  267.4 2.1 copy-start.3
  294.1 2.1 copy-start.3
  320.9 2.1 copy-start.3
  348.0 2.1 copy-start.3
  375.0 2.1 copy-start.3
  401.9 2.1 copy-start.3
  412.3 45.6 %collective-permute-start.2 = (bf16[12,32768]{1,0:T(8,128)(2,1)}, bf16[12,32768]{1,0:T(8,128)(2,1)}, u32[]{:S(2)}, u32[]{:S(2)}) collective-permute-start(bf16[12,32768]{1,0:T(8,128)(2,1)} %convert_element_type.89), channel_id=1, source_target_pairs={{2,0},{4,2},{6,4},{8,6},{10,8},{12,10},{14,12},{16,14},{18,16},{20... | collective-permute-start | bytes 2359304 | tf_op jit(solution)/shard_map/ppermute | solution.py:19
  428.4 4.7 copy-start.11
  440.8 4.0 slice-start
  456.0 60.3 %collective-permute-start.3 = (bf16[12,32768]{1,0:T(8,128)(2,1)}, bf16[12,32768]{1,0:T(8,128)(2,1)}, u32[]{:S(2)}, u32[]{:S(2)}) collective-permute-start(bf16[12,32768]{1,0:T(8,128)(2,1)} %convert_element_type.92), channel_id=1, source_target_pairs={{2,0},{4,2},{6,4},{8,6},{10,8},{12,10},{14,12},{16,14},{18,16},{20... | collective-permute-start | bytes 2359304 | tf_op jit(solution)/shard_map/ppermute | solution.py:19
  457.8 5.3 %copy-start.1 = (bf16[640,768]{0,1:T(8,128)(2,1)S(1)}, bf16[640,768]{0,1:T(8,128)(2,1)}, u32[]{:S(2)}) copy-start(bf16[640,768]{0,1:T(8,128)(2,1)} %copy-done) | copy-start | bytes 2949124
  457.8 5.3 %copy-start.8 = (f32[12,640]{1,0:T(8,128)S(1)}, f32[12,640]{1,0:T(8,128)}, u32[]{:S(2)}) copy-start(f32[12,640]{1,0:T(8,128)} %copy-done.7) | copy-start | bytes 92164
  457.8 5.3 %copy-start.10 = (f32[12,640]{1,0:T(8,128)S(1)}, f32[12,640]{1,0:T(8,128)}, u32[]{:S(2)}) copy-start(f32[12,640]{1,0:T(8,128)} %copy-done.9) | copy-start | bytes 92164
  457.9 5.3 %copy-start.15 = (f32[64]{0:T(128)S(1)}, f32[64]{0:T(128)}, u32[]{:S(2)}) copy-start(f32[64]{0:T(128)} %copy-done.14) | copy-start | bytes 772
  463.1 3.6 copy-start.2
  (13 other events, 15.2 us)
where the time goes:
time: 534 us; the launch traced here: 525 us
  local copies, waits for them, and re-layouts  345 us (65%)
  matrix products  68.1 us (13%)
  other arithmetic  55.5 us (10%)
  blocking collectives  41.8 us (8%)
  starting transfers between devices  10.7 us (2%)
    concatenate x24, local copies, waits for them, and re-layouts, band_of(): jnp.concatenate([segments[offset:offset + seg_count] for offset in range(...  73.8 us
    slice x12, local copies, waits for them, and re-layouts, band_of(): segments[offset:offset + seg_count]  49 us
    psum x1, blocking collectives, body(): lax.psum((full_table, query_gain_part, key_gain_part), ('sp', 'tp'))  41.8 us
    dynamic_update_slice x60, local copies, waits for them, and re-layouts, body(): lax.map(main_head, (query_unit, cotangent_heads, key_ext, value_ext, bias...  38.9 us
    dynamic_slice x36, local copies, waits for them, and re-layouts, body(): lax.map(main_head, (query_unit, cotangent_heads, key_ext, value_ext, bias...  30.8 us
    unnamed x48, local copies, waits for them, and re-layouts  27.6 us
    scatter-add x192, other arithmetic, unband(): summed.at[offset:offset + seg_count]  22.9 us
    dot_general x12, matrix products, backward_block(): jnp.einsum('cqd,ckd->cqk', grad_seg, value_band, preferred_element_type=j...  21.1 us
  transfers between devices with their start and end apart: 4, of which 0 were waited for; matrix products, arithmetic and copies ran while one was open for 20% of the time, Pallas kernels for 0%

commit v1 on v0

v1 whole, which is shorter than its diff:
```python
import functools

import jax
import jax.numpy as jnp
from jax import lax
from jax.experimental import pallas as pl
from jax.experimental.pallas import tpu as pltpu
from jax.sharding import PartitionSpec as P

SEG = 64
LEFT = 8
REACH = SEG * LEFT
RSPAN = 320
NORM_EPS = 1e-06
BLK = 2 * SEG
BAND = REACH + BLK
NEG = -1e30
F32 = jnp.float32
BF16 = jnp.bfloat16


def dot(a, b, dims):
    return lax.dot_general(a, b, (dims, ((), ())), preferred_element_type=F32)


def half_ones():
    row = lax.broadcasted_iota(jnp.int32, (BLK, BLK), 0) // 64
    col = lax.broadcasted_iota(jnp.int32, (BLK, BLK), 1) // 64
    return jnp.where(row == col, 1.0, 0.0).astype(BF16)


def head_mean(x, ones):
    high = x.astype(BF16)
    low = (x - high.astype(F32)).astype(BF16)
    return (dot(high, ones, ((1,), (0,))) + dot(low, ones, ((1,), (0,)))) * (1.0 / 64.0)


def normed(rows, ones):
    wide = rows.astype(F32)
    scale = lax.rsqrt(head_mean(wide * wide, ones) + NORM_EPS)
    return wide * scale, scale


def norm_grad(d_unit, gain, hat, scale, ones):
    scaled = d_unit * gain
    return scale * (scaled - hat * head_mean(scaled * hat, ones))


def stack_halves(x):
    lane = lax.broadcasted_iota(jnp.int32, x.shape, 1)
    zero = jnp.zeros_like(x)
    return jnp.concatenate([jnp.where(lane < 64, x, zero), jnp.where(lane < 64, zero, x)], axis=0)


def build_bias(table_row, bias_ref, head):
    wide = jnp.broadcast_to(table_row, (8, 512))
    sub = lax.broadcasted_iota(jnp.int32, (8, 512), 0)
    for bit in (1, 2, 4):
        wide = jnp.where((sub & bit) != 0, pltpu.roll(wide, bit, 1), wide)
    half = 8
    while half < BLK:
        wide = jnp.concatenate([wide, pltpu.roll(wide, half, 1)], axis=0)
        half *= 2
    lanes = slice(head * BLK, (head + 1) * BLK)
    row = lax.broadcasted_iota(jnp.int32, (BLK, BLK), 0)
    col = lax.broadcasted_iota(jnp.int32, (BLK, BLK), 1)
    far = jnp.broadcast_to(table_row[:, 0:1], (BLK, BLK))
    bias_ref[0:BLK, lanes] = jnp.where((row < SEG) & (col >= SEG), NEG, far)
    bias_ref[BLK : 2 * BLK, lanes] = far
    for j in range(3):
        tile = wide[:, ((4 - j) % 4) * BLK : ((4 - j) % 4) * BLK + BLK]
        if j == 2:
            tile = jnp.where((row >= SEG) & (col < SEG), NEG, tile)
        bias_ref[(2 + j) * BLK : (3 + j) * BLK, lanes] = tile


def fold_bias(acc_ref, head):
    lanes = slice(head * BLK, (head + 1) * BLK)
    tiles = [acc_ref[j * BLK : (j + 1) * BLK, lanes] for j in range(3)]
    wide = jnp.concatenate([tiles[0], jnp.zeros_like(tiles[0]), tiles[2], tiles[1]], axis=1)
    half = BLK // 2
    while half >= 8:
        wide = wide[:half] + pltpu.roll(wide[half:], 512 - half, 1)
        half //= 2
    for half in (4, 2, 1):
        wide = wide + pltpu.roll(pltpu.roll(wide, 512 - half, 1), 8 - half, 0)
    return wide[0:1]


def attend(refs, first, blocks, ones, gain_q):
    (q_ref, g_ref, qg_ref, gq_ref, clip_ref, k_s, kt_s, v_s, bias_s, acc_s, s_s, dw_s, w_s, ds_s, dk_s, dv_s) = refs

    def block(i, _):
        base = pl.multiple_of(i * BLK, BLK)
        rows = pl.ds(base, BLK)
        hat, scale = normed(q_ref[rows, :], ones)
        qs = stack_halves((hat * gain_q).astype(BF16) * jnp.asarray(0.125, BF16))
        gs = stack_halves(g_ref[rows, :])
        peaks, penalties = [], []
        for j in range(5):
            keys = pl.ds(base + j * BLK, BLK)
            own = slice(j * BLK, (j + 1) * BLK)
            s = dot(k_s[keys, :], qs, ((1,), (1,))) + bias_s[own, :]
            s_s[own, :] = s
            dw_s[own, :] = dot(v_s[keys, :], gs, ((1,), (1,)))
            penalty = jnp.where(first & (j < 4 - i), NEG, 0.0)
            penalties.append(penalty)
            peaks.append(jnp.max(s, axis=0, keepdims=True) + penalty)
        peak = functools.reduce(jnp.maximum, peaks)
        total = jnp.zeros((1, 2 * BLK), F32)
        delta = jnp.zeros((1, 2 * BLK), F32)
        for j in range(5):
            own = slice(j * BLK, (j + 1) * BLK)
            e = jnp.exp(s_s[own, :] - (peak - penalties[j]))
            s_s[own, :] = e
            total = total + jnp.sum(e, axis=0, keepdims=True)
            delta = delta + jnp.sum(e * dw_s[own, :], axis=0, keepdims=True)
        inverse = 1.0 / total
        delta = delta * inverse
        clipped = jnp.zeros((1, 2 * BLK), F32)
        for j in range(5):
            own = slice(j * BLK, (j + 1) * BLK)
            keys = pl.ds(base + j * BLK, BLK)
            w = s_s[own, :] * inverse
            ds = w * (dw_s[own, :] - delta)
            if j < 2:
                clipped = clipped + jnp.sum(ds, axis=0, keepdims=True)
            else:
                acc_s[(j - 2) * BLK : (j - 1) * BLK, :] += ds
            w_low = w.astype(BF16)
            ds_low = ds.astype(BF16)
            ds_s[own, :] = ds_low
            dk_s[keys, :] += dot(ds_low, qs, ((1,), (0,)))
            dv_s[keys, :] += dot(w_low, gs, ((1,), (0,)))
        clip_ref[...] += clipped
        dqt = dot(kt_s[:, pl.ds(base, BAND)], ds_s[...], ((1,), (0,)))
        dqt = jnp.concatenate([dqt[:64, :BLK], dqt[64:, BLK:]], axis=0)
        dq = dqt.T * 0.125
        gq_ref[...] += jnp.sum(dq * hat, axis=0, keepdims=True)
        qg_ref[rows, :] = norm_grad(dq, gain_q, hat, scale, ones).astype(BF16)
        return 0

    lax.fori_loop(0, blocks, block, 0)


def main_kernel(
    q_ref, k_ref, v_ref, g_ref, pk_ref, pv_ref, gains_ref, table_ref,
    qg_ref, dk_ref, dv_ref, ck_ref, cv_ref, bg_ref, clip_ref, gq_ref,
    k_s, kt_s, v_s, bias_s, acc_s, s_s, dw_s, w_s, ds_s, dk_s, dv_s,
):
    tokens = q_ref.shape[0]
    first = lax.axis_index("sp") == 0
    ones = half_ones()
    gain_q = gains_ref[0:1, :]
    gain_k = gains_ref[1:2, :]
    for b in range((tokens + REACH) // BLK):
        raw = pk_ref[b * BLK : (b + 1) * BLK, :] if b < 4 else k_ref[(b - 4) * BLK : (b - 3) * BLK, :]
        unit = normed(raw, ones)[0] * gain_k
        k_s[b * BLK : (b + 1) * BLK, :] = unit.astype(BF16)
        kt_s[:, b * BLK : (b + 1) * BLK] = unit.T.astype(BF16)
    v_s[:REACH, :] = pv_ref[...]
    v_s[REACH:, :] = v_ref[...]
    dk_s[...] = jnp.zeros_like(dk_s)
    dv_s[...] = jnp.zeros_like(dv_s)
    acc_s[...] = jnp.zeros_like(acc_s)
    clip_ref[...] = jnp.zeros_like(clip_ref)
    gq_ref[...] = jnp.zeros_like(gq_ref)
    for head in range(2):
        build_bias(table_ref[head : head + 1, :], bias_s, head)
    attend(
        (q_ref, g_ref, qg_ref, gq_ref, clip_ref, k_s, kt_s, v_s, bias_s, acc_s, s_s, dw_s, w_s, ds_s, dk_s, dv_s),
        first, tokens // BLK, ones, gain_q,
    )
    for head in range(2):
        bg_ref[head : head + 1, :] = fold_bias(acc_s, head)
    ck_ref[...] = dk_s[:REACH, :].astype(BF16)
    cv_ref[...] = dv_s[:REACH, :].astype(BF16)
    dk_ref[...] = dk_s[REACH:, :]
    dv_ref[...] = dv_s[REACH:, :]


def final_kernel(k_ref, dk_ref, dv_ref, bk_ref, bv_ref, gains_ref, kg_ref, vg_ref, gk_ref):
    tokens = k_ref.shape[0]
    ones = half_ones()
    gain_k = gains_ref[1:2, :]
    total = jnp.zeros((1, BLK), F32)
    for b in range(tokens // BLK):
        rows = slice(b * BLK, (b + 1) * BLK)
        hat, scale = normed(k_ref[rows, :], ones)
        dk, dv = dk_ref[rows, :], dv_ref[rows, :]
        back = b * BLK - (tokens - REACH)
        if back >= 0:
            dk = dk + bk_ref[back : back + BLK, :].astype(F32)
            dv = dv + bv_ref[back : back + BLK, :].astype(F32)
        total = total + jnp.sum(dk * hat, axis=0, keepdims=True)
        kg_ref[rows, :] = norm_grad(dk, gain_k, hat, scale, ones).astype(BF16)
        vg_ref[rows, :] = dv.astype(BF16)
    gk_ref[...] = total


def passed_along(block, axis, distance):
    devices = range(lax.axis_size(axis))
    route = [(i - distance, i) for i in devices if i - distance in devices]
    return lax.ppermute(block, axis, route)


def body(query_rows, key_rows, value_rows, query_gain, key_gain, position_bias, output_grad):
    heads = position_bias.shape[0]
    pairs = heads // 2
    tokens = query_rows.shape[0]
    table = position_bias.astype(F32)
    last = jnp.broadcast_to(table[:, -1:], (heads, 129))
    table = jnp.concatenate([last, jnp.full((heads, 64), NEG, F32), table[:, :-1]], axis=1)
    table = table.reshape(pairs, 2, 512)
    gains = jnp.stack([jnp.tile(query_gain.astype(F32), 2), jnp.tile(key_gain.astype(F32), 2)])
    prior_key, prior_value = passed_along((key_rows[tokens - REACH :], value_rows[tokens - REACH :]), "sp", 1)

    full = pl.BlockSpec((tokens, BLK), lambda p: (0, p))
    reach = pl.BlockSpec((REACH, BLK), lambda p: (0, p))
    small = pl.BlockSpec((2, BLK), lambda p: (0, 0))

    def per_pair(rows, lanes):
        return pl.BlockSpec((None, rows, lanes), lambda p: (p, 0, 0))

    def shape(rows, dtype):
        return jax.ShapeDtypeStruct((rows, heads * 64), dtype)

    flops = pairs * tokens * 2 * 5 * 2 * BAND * 128
    ext = tokens + REACH
    query_grad, dk_own, dv_own, cross_k, cross_v, fold, clip, gq = pl.pallas_call(
        main_kernel,
        grid=(pairs,),
        in_specs=[full, full, full, full, reach, reach, small, per_pair(2, 512)],
        out_specs=[full, full, full, reach, reach, per_pair(2, 512), per_pair(1, 2 * BLK), per_pair(1, BLK)],
        out_shape=[
            shape(tokens, BF16), shape(tokens, F32), shape(tokens, F32), shape(REACH, BF16), shape(REACH, BF16),
            jax.ShapeDtypeStruct((pairs, 2, 512), F32),
            jax.ShapeDtypeStruct((pairs, 1, 2 * BLK), F32),
            jax.ShapeDtypeStruct((pairs, 1, BLK), F32),
        ],
        scratch_shapes=[
            pltpu.VMEM((ext, BLK), BF16), pltpu.VMEM((BLK, ext), BF16), pltpu.VMEM((ext, BLK), BF16),
            pltpu.VMEM((BAND, 2 * BLK), F32), pltpu.VMEM((3 * BLK, 2 * BLK), F32),
            pltpu.VMEM((BAND, 2 * BLK), F32), pltpu.VMEM((BAND, 2 * BLK), F32),
            pltpu.VMEM((BAND, 2 * BLK), BF16), pltpu.VMEM((BAND, 2 * BLK), BF16),
            pltpu.VMEM((ext, BLK), F32), pltpu.VMEM((ext, BLK), F32),
        ],
        cost_estimate=pl.CostEstimate(flops=flops, bytes_accessed=14_000_000, transcendentals=pairs * tokens * BAND),
        name="attend",
    )(query_rows, key_rows, value_rows, output_grad, prior_key, prior_value, gains, table)

    back_k, back_v = passed_along((cross_k, cross_v), "sp", -1)
    key_grad, value_grad, gk = pl.pallas_call(
        final_kernel,
        grid=(pairs,),
        in_specs=[full, full, full, reach, reach, small],
        out_specs=[full, full, per_pair(1, BLK)],
        out_shape=[shape(tokens, BF16), shape(tokens, BF16), jax.ShapeDtypeStruct((pairs, 1, BLK), F32)],
        name="finish",
    )(key_rows, dk_own, dv_own, back_k, back_v, gains)

    fold = fold.reshape(heads, 512)
    clip = jnp.sum(clip.reshape(heads, BLK), axis=1, keepdims=True)
    bias_part = jnp.concatenate([fold[:, 193:], jnp.sum(fold[:, :129], axis=1, keepdims=True) + clip], axis=1)
    gain_part = jnp.stack([jnp.sum(x.reshape(-1, 64), axis=0) for x in (gq, gk)])
    bias_grad = lax.psum(bias_part, "sp")
    gain_grad = lax.psum(gain_part, ("sp", "tp"))
    return (query_grad, key_grad, value_grad, bias_grad, gain_grad[0], gain_grad[1])


def solution(mesh):
    placed = (P("sp", "tp"), P("sp", "tp"), P("sp", "tp"), P(), P(), P("tp", None), P("sp", "tp"))
    return jax.shard_map(
        body,
        mesh=mesh,
        in_specs=placed,
        out_specs=(P("sp", "tp"), P("sp", "tp"), P("sp", "tp"), P("tp", None), P(), P()),
        check_vma=False,
    )
```

time: 534 us -> 195 us (0.37); the launches traced: 525 us -> 194 us
  local copies, waits for them, and re-layouts: 345 us -> 6.95 us
  blocking collectives: 41.8 us -> 117 us
  matrix products: 68.1 us -> 0 us
  Pallas kernels: 0 us -> 56.1 us
  other arithmetic: 55.5 us -> 3.15 us
    slice x55 -> x5, local copies, waits for them, and re-layouts: 85.2 us -> 1.58 us  [the longest x1 1.27 us: body(): key_rows[tokens - REACH:]]
    psum x1 -> x2, blocking collectives: 41.8 us -> 117 us  [the longest x1 80.2 us: body(): bias_grad = lax.psum(bias_part, 'sp')]
    concatenate x24 -> x1, local copies, waits for them, and re-layouts: 73.8 us -> 0.08 us  [body(): jnp.concatenate([last, jnp.full((heads, 64), NEG, F32), table[:, :-1]], a...]
    pallas_call x0 -> x2, Pallas kernels: none -> 56.1 us  [the longest x1 49.3 us: body(): pl.pallas_call(main_kernel, grid=(pairs,), in_specs=[full, full, full, fu...]
    dot_general x48 -> x0, matrix products: 47.6 us -> none  [the longest x12 21.1 us: backward_block(): jnp.einsum('cqd,ckd->cqk', grad_seg, value_band, preferred_element_type=j...]
    reshape x11 -> x5, local copies, waits for them, and re-layouts: 41.2 us -> 1.53 us  [the longest x1 0.75 us: body(): fold = fold.reshape(heads, 512)]
    dynamic_update_slice x61 -> x0, local copies, waits for them, and re-layouts: 39.4 us -> none  [the longest x60 38.9 us: body(): lax.map(main_head, (query_unit, cotangent_heads, key_ext, value_ext, bias...]
    dynamic_slice x37 -> x0, local copies, waits for them, and re-layouts: 31.4 us -> none  [the longest x36 30.8 us: body(): lax.map(main_head, (query_unit, cotangent_heads, key_ext, value_ext, bias...]
  transfers between devices with their start and end apart: 4 -> 4, of which waited for: 0 -> 0; matrix products, arithmetic and copies ran while one was open for 20% -> 2% of each run, Pallas kernels for 0% -> 0%
where the time goes in v1:
time: 195 us; the launch traced here: 194 us
  blocking collectives  117 us (60%)
  Pallas kernels  56.1 us (29%)
  starting transfers between devices  9.56 us (5%)
  local copies, waits for them, and re-layouts  6.95 us (4%)
  other arithmetic  3.15 us (2%)
    psum x1, blocking collectives, body(): bias_grad = lax.psum(bias_part, 'sp')  80.2 us
    pallas_call x1, Pallas kernels, body(): pl.pallas_call(main_kernel, grid=(pairs,), in_specs=[full, full, full, fu...  49.3 us
    psum x1, blocking collectives, body(): gain_grad = lax.psum(gain_part, ('sp', 'tp'))  36.8 us
    ppermute x4, starting transfers between devices, passed_along(): return lax.ppermute(block, axis, route)  9.56 us
    pallas_call x1, Pallas kernels, body(): pl.pallas_call(final_kernel, grid=(pairs,), in_specs=[full, full, full, r...  6.77 us
  transfers between devices with their start and end apart: 4, of which 0 were waited for; matrix products, arithmetic and copies ran while one was open for 2% of the time, Pallas kernels for 0%

profile of v1, /device:TPU:0, one launch (start us, length us, event | category | flops | bytes accessed | tf_op | source)
XLA Modules:
  0.0 193.6 jit_solution(15721880746529279836)
XLA Ops:
  0.7 1.3 slice.24
  1.9 2.4 %collective-permute-start = (bf16[512,768]{1,0:T(8,128)(2,1)S(1)}, bf16[512,768]{1,0:T(8,128)(2,1)S(1)}, u32[]{:S(2)}, u32[]{:S(2)}) collective-permute-start(bf16[512,768]{1,0:T(8,128)(2,1)S(1)} %slice.24), channel_id=1, source_target_pairs={{0,2},{2,4},{4,6},{6,8},{8,10},{10,12},{12,14},{14,16},{16,18},{18... | collective-permute-start | bytes 2359304 | tf_op jit(solution)/shard_map/ppermute | solution.py:204
  4.5 4.5 %collective-permute-start.1 = (bf16[512,768]{1,0:T(8,128)(2,1)S(1)}, bf16[512,768]{1,0:T(8,128)(2,1)S(1)}, u32[]{:S(2)}, u32[]{:S(2)}) collective-permute-start(bf16[512,768]{1,0:T(8,128)(2,1)S(1)} %slice.25), channel_id=1, source_target_pairs={{0,2},{2,4},{4,6},{6,8},{8,10},{10,12},{12,14},{14,16},{16,18},{18... | collective-permute-start | bytes 2359304 | tf_op jit(solution)/shard_map/ppermute | solution.py:204
  9.1 0.1 stack_tile.6
  9.1 0.1 stack_tile.7
  9.2 0.1 pad.5.clone
  9.3 0.2 slice_reduce_fusion.1
  9.5 0.1 broadcast_in_dim.13
  9.6 0.1 pad_maximum_fusion
  9.6 0.6 reshape.42.table_ref
  10.3 0.6 pad_maximum_fusion.2.gains_ref
  10.9 0.9 copy-done.4
  11.8 0.9 copy-done.5
  12.6 49.3 %attend.1 = (bf16[640,768]{1,0:T(8,128)(2,1)}, f32[640,768]{1,0:T(8,128)}, f32[640,768]{1,0:T(8,128)}, bf16[512,768]{1,0:T(8,128)(2,1)}, bf16[512,768]{1,0:T(8,1...) custom-call(bf16[640,768]{1,0:T(8,128)(2,1)} %q_ref.1, bf16[640,768]{1,0:T(8,128)(2,1)} %k_ref.3, ...), custom_call_target="tpu_custom_call" | custom-call | flops 6291456000 | bytes 14000000 | tf_op jit(solution)/shard_map/attend/pallas_call | solution.py:230
  62.0 1.3 collective-permute-start.2
  63.3 1.3 collective-permute-start.3
  64.6 0.7 reduce.2
  65.3 0.1 reshape.45
  65.3 0.7 reduce.1
  66.1 0.1 reduce_sum.37
  66.2 0.8 reshape.43
  67.0 0.1 slice.34
  67.0 0.1 slice_reduce_fusion
  67.1 0.1 copy.14
  67.2 0.1 pad_maximum_fusion.1
  67.3 80.2 %psum.14 = f32[12,320]{1,0:T(8,128)} all-reduce(f32[12,320]{1,0:T(8,128)S(1)} %pad_maximum_fusion.1), channel_id=1, replica_groups=mesh['sp'=16,'tp'=2] {'sp'}, use_global_device_ids=true, to_apply=%region_2.0 | all-reduce | flops 3840 | bytes 30720 | tf_op jit(solution)/shard_map/psum | solution.py:266
  147.5 0.9 copy-done
  148.4 0.3 copy-done.1
  148.7 6.8 %finish.1 = (bf16[640,768]{1,0:T(8,128)(2,1)}, bf16[640,768]{1,0:T(8,128)(2,1)}, f32[6,1,128]{2,1,0:T(1,128)}) custom-call(bf16[640,768]{1,0:T(8,128)(2,1)} %k_ref.3, f32[640,768]{1,0:T(8,128)} %get-tuple-element.18.dk_ref, f32[640,768]{1,0:T(8,128)} %get-tuple-element.19.dv_ref, bf16[512,768]{1,0:T(8,128)(2,1)} %copy-done, bf16[512,768]{1,0:T(8,128)(2,1)} %copy-done.1, ...), custom_call_target="tpu_custom_call" | custom-call | tf_op jit(solution)/shard_map/finish/pallas_call | solution.py:253
  155.4 0.7 reduce.3
  156.2 36.8 %psum.15 = f32[2,64]{1,0:T(2,128)S(1)} all-reduce(f32[2,64]{1,0:T(2,128)S(1)} %pad_maximum_fusion.3), channel_id=1, replica_groups=mesh['sp'=16,'tp'=2] {'sp','tp'}, use_global_device_ids=true, to_apply=%region_5.0 | all-reduce | flops 128 | bytes 1024 | tf_op jit(solution)/shard_map/psum | solution.py:267
  193.1 0.5 slice_bitcast_fusion
  (28 shorter events, 0.2 us)
Async XLA Ops:
  0.6 3.8 %copy-start.2 = (bf16[640,768]{1,0:T(8,128)(2,1)S(1)}, bf16[640,768]{1,0:T(8,128)(2,1)}, u32[]{:S(2)}) copy-start(bf16[640,768]{1,0:T(8,128)(2,1)} %v_ref.1) | copy-start | bytes 2949124
  0.6 8.4 %copy-start.3 = (bf16[12,320]{1,0:T(8,128)(2,1)S(1)}, bf16[12,320]{1,0:T(8,128)(2,1)}, u32[]{:S(2)}) copy-start(bf16[12,320]{1,0:T(8,128)(2,1)} %param.12) | copy-start | bytes 23044
  0.7 8.4 %copy-start.6 = (bf16[64]{0:T(256)(128)(2,1)S(1)}, bf16[64]{0:T(256)(128)(2,1)}, u32[]{:S(2)}) copy-start(bf16[64]{0:T(256)(128)(2,1)} %param.10) | copy-start | bytes 388
  0.7 8.5 %copy-start.7 = (bf16[64]{0:T(256)(128)(2,1)S(1)}, bf16[64]{0:T(256)(128)(2,1)}, u32[]{:S(2)}) copy-start(bf16[64]{0:T(256)(128)(2,1)} %param.11) | copy-start | bytes 388
  1.9 8.9 %collective-permute-start = (bf16[512,768]{1,0:T(8,128)(2,1)S(1)}, bf16[512,768]{1,0:T(8,128)(2,1)S(1)}, u32[]{:S(2)}, u32[]{:S(2)}) collective-permute-start(bf16[512,768]{1,0:T(8,128)(2,1)S(1)} %slice.24), channel_id=1, source_target_pairs={{0,2},{2,4},{4,6},{6,8},{8,10},{10,12},{12,14},{14,16},{16,18},{18... | collective-permute-start | bytes 2359304 | tf_op jit(solution)/shard_map/ppermute | solution.py:204
  4.5 6.4 %collective-permute-start.1 = (bf16[512,768]{1,0:T(8,128)(2,1)S(1)}, bf16[512,768]{1,0:T(8,128)(2,1)S(1)}, u32[]{:S(2)}, u32[]{:S(2)}) collective-permute-start(bf16[512,768]{1,0:T(8,128)(2,1)S(1)} %slice.25), channel_id=1, source_target_pairs={{0,2},{2,4},{4,6},{6,8},{8,10},{10,12},{12,14},{14,16},{16,18},{18... | collective-permute-start | bytes 2359304 | tf_op jit(solution)/shard_map/ppermute | solution.py:204
  10.9 0.9 copy-start.4
  11.8 0.9 copy-start.5
  62.0 85.6 %collective-permute-start.2 = (bf16[512,768]{1,0:T(8,128)(2,1)}, bf16[512,768]{1,0:T(8,128)(2,1)S(1)}, u32[]{:S(2)}, u32[]{:S(2)}) collective-permute-start(bf16[512,768]{1,0:T(8,128)(2,1)} %get-tuple-element.20), channel_id=1, source_target_pairs={{2,0},{4,2},{6,4},{8,6},{10,8},{12,10},{14,12},{16,14},{18,16},{20... | collective-permute-start | bytes 2359304 | tf_op jit(solution)/shard_map/ppermute | solution.py:204
  63.3 84.3 %collective-permute-start.3 = (bf16[512,768]{1,0:T(8,128)(2,1)}, bf16[512,768]{1,0:T(8,128)(2,1)S(1)}, u32[]{:S(2)}, u32[]{:S(2)}) collective-permute-start(bf16[512,768]{1,0:T(8,128)(2,1)} %get-tuple-element.21), channel_id=1, source_target_pairs={{2,0},{4,2},{6,4},{8,6},{10,8},{12,10},{14,12},{16,14},{18,16},{20... | collective-permute-start | bytes 2359304 | tf_op jit(solution)/shard_map/ppermute | solution.py:204
  147.5 0.9 copy-start
  147.5 1.1 copy-start.1

commit v2 on v1

v2 whole, which is shorter than its diff:
```python
import functools

import jax
import jax.numpy as jnp
from jax import lax
from jax.experimental import pallas as pl
from jax.experimental.pallas import tpu as pltpu
from jax.sharding import PartitionSpec as P

SEG = 64
LEFT = 8
REACH = SEG * LEFT
RSPAN = 320
NORM_EPS = 1e-06
BLK = 2 * SEG
BAND = REACH + BLK
NEG = -1e30
F32 = jnp.float32
BF16 = jnp.bfloat16


def dot(a, b, dims):
    return lax.dot_general(a, b, (dims, ((), ())), preferred_element_type=F32)


def half_ones():
    row = lax.broadcasted_iota(jnp.int32, (BLK, BLK), 0) // 64
    col = lax.broadcasted_iota(jnp.int32, (BLK, BLK), 1) // 64
    return jnp.where(row == col, 1.0, 0.0).astype(BF16)


def head_mean(x, ones):
    high = x.astype(BF16)
    low = (x - high.astype(F32)).astype(BF16)
    return (dot(high, ones, ((1,), (0,))) + dot(low, ones, ((1,), (0,)))) * (1.0 / 64.0)


def normed(rows, ones):
    wide = rows.astype(F32)
    scale = lax.rsqrt(head_mean(wide * wide, ones) + NORM_EPS)
    return wide * scale, scale


def norm_grad(d_unit, gain, hat, scale, ones):
    scaled = d_unit * gain
    return scale * (scaled - hat * head_mean(scaled * hat, ones))


def stack_halves(x):
    lane = lax.broadcasted_iota(jnp.int32, x.shape, 1)
    zero = jnp.zeros_like(x)
    return jnp.concatenate([jnp.where(lane < 64, x, zero), jnp.where(lane < 64, zero, x)], axis=0)


def build_bias(table_row, bias_ref, head):
    wide = jnp.broadcast_to(table_row, (8, 512))
    sub = lax.broadcasted_iota(jnp.int32, (8, 512), 0)
    for bit in (1, 2, 4):
        wide = jnp.where((sub & bit) != 0, pltpu.roll(wide, bit, 1), wide)
    half = 8
    while half < BLK:
        wide = jnp.concatenate([wide, pltpu.roll(wide, half, 1)], axis=0)
        half *= 2
    lanes = slice(head * BLK, (head + 1) * BLK)
    row = lax.broadcasted_iota(jnp.int32, (BLK, BLK), 0)
    col = lax.broadcasted_iota(jnp.int32, (BLK, BLK), 1)
    far = jnp.broadcast_to(table_row[:, 0:1], (BLK, BLK))
    bias_ref[0:BLK, lanes] = jnp.where((row < SEG) & (col >= SEG), NEG, far)
    bias_ref[BLK : 2 * BLK, lanes] = far
    for j in range(3):
        tile = wide[:, ((4 - j) % 4) * BLK : ((4 - j) % 4) * BLK + BLK]
        if j == 2:
            tile = jnp.where((row >= SEG) & (col < SEG), NEG, tile)
        bias_ref[(2 + j) * BLK : (3 + j) * BLK, lanes] = tile


def fold_bias(acc_ref, head):
    lanes = slice(head * BLK, (head + 1) * BLK)
    tiles = [acc_ref[j * BLK : (j + 1) * BLK, lanes] for j in range(3)]
    wide = jnp.concatenate([tiles[0], jnp.zeros_like(tiles[0]), tiles[2], tiles[1]], axis=1)
    half = BLK // 2
    while half >= 8:
        wide = wide[:half] + pltpu.roll(wide[half:], 512 - half, 1)
        half //= 2
    for half in (4, 2, 1):
        wide = wide + pltpu.roll(pltpu.roll(wide, 512 - half, 1), 8 - half, 0)
    return wide[0:1]


def flip(index, distance):
    return index + distance * (1 - 2 * ((index // distance) % 2))


def doubling(size):
    return [1 << r for r in range(size.bit_length() - 1)]


def kernel(
    sp, tp, q_ref, k_ref, v_ref, g_ref, gains_ref, table_ref,
    qg_ref, kg_ref, vg_ref, out_ref,
    k_s, kt_s, v_s, bias_s, acc_s, s_s, dw_s, ds_s, dk_s, dv_s, clip_s, gq_s, gk_s,
    pk_s, pv_s, ck_s, cv_s, bk_s, bv_s, stat_s, got_s,
    prior_send, prior_recv, cross_send, cross_recv, stat_send, stat_recv,
):
    tokens = q_ref.shape[0]
    blocks = tokens // BLK
    pairs = pk_s.shape[0]
    me = lax.axis_index("sp")
    me_tp = lax.axis_index("tp")
    right, left = lax.rem(me + 1, sp), lax.rem(me + sp - 1, sp)
    partners = [{"sp": flip(me, d)} for d in doubling(sp)] + [{"tp": flip(me_tp, d)} for d in doubling(tp)]
    first = me == 0

    barrier = pltpu.get_barrier_semaphore()
    greeted = [{"sp": right}, {"sp": left}] + partners
    for device in greeted:
        pl.semaphore_signal(barrier, inc=1, device_id=device, device_id_type=pl.DeviceIdType.MESH)
    pl.semaphore_wait(barrier, len(greeted))

    def remote(src, dst, send, recv, device):
        return pltpu.make_async_remote_copy(
            src_ref=src, dst_ref=dst, send_sem=send, recv_sem=recv,
            device_id=device, device_id_type=pl.DeviceIdType.MESH,
        )

    def lanes_of(p):
        return pl.ds(pl.multiple_of(p * BLK, BLK), BLK)

    def prior_copies(p):
        rows = slice(tokens - REACH, tokens)
        return (
            remote(k_ref.at[rows, lanes_of(p)], pk_s.at[p], prior_send.at[0, p], prior_recv.at[0, p], {"sp": right}),
            remote(v_ref.at[rows, lanes_of(p)], pv_s.at[p], prior_send.at[1, p], prior_recv.at[1, p], {"sp": right}),
        )

    def cross_copies(p):
        return (
            remote(ck_s.at[p], bk_s.at[p], cross_send.at[0, p], cross_recv.at[0, p], {"sp": left}),
            remote(cv_s.at[p], bv_s.at[p], cross_send.at[1, p], cross_recv.at[1, p], {"sp": left}),
        )

    for p in range(pairs):
        for copy in prior_copies(p):
            copy.start()

    ones = half_ones()
    gain_q = gains_ref[0:1, :]
    gain_k = gains_ref[1:2, :]
    stat_s[0] = jnp.zeros(stat_s.shape[1:], F32)
    gq_s[...] = jnp.zeros_like(gq_s)
    gk_s[...] = jnp.zeros_like(gk_s)

    def key_tile(raw, b):
        unit = normed(raw, ones)[0] * gain_k
        k_s[b * BLK : (b + 1) * BLK, :] = unit.astype(BF16)
        kt_s[:, b * BLK : (b + 1) * BLK] = unit.T.astype(BF16)

    def finish(p):
        slot = lax.rem(p, 2)
        for copy in cross_copies(p):
            copy.wait_recv()
        total = jnp.zeros((1, BLK), F32)
        for b in range(blocks):
            rows = slice(b * BLK, (b + 1) * BLK)
            hat, scale = normed(k_ref[rows, lanes_of(p)], ones)
            ext = slice(REACH + b * BLK, REACH + (b + 1) * BLK)
            dk, dv = dk_s[slot, ext, :], dv_s[slot, ext, :]
            back = b * BLK - (tokens - REACH)
            if back >= 0:
                dk = dk + bk_s[p, back : back + BLK, :].astype(F32)
                dv = dv + bv_s[p, back : back + BLK, :].astype(F32)
            total = total + jnp.sum(dk * hat, axis=0, keepdims=True)
            kg_ref[rows, lanes_of(p)] = norm_grad(dk, gain_k, hat, scale, ones).astype(BF16)
            vg_ref[rows, lanes_of(p)] = dv.astype(BF16)
        gk_s[...] += total

    def pair(p, _):
        slot = lax.rem(p, 2)
        for b in range(blocks):
            key_tile(k_ref[b * BLK : (b + 1) * BLK, lanes_of(p)], b + LEFT // 2)
        v_s[REACH:, :] = v_ref[:, lanes_of(p)]
        dk_s[slot] = jnp.zeros(dk_s.shape[1:], F32)
        dv_s[slot] = jnp.zeros(dv_s.shape[1:], F32)
        acc_s[...] = jnp.zeros_like(acc_s)
        clip_s[...] = jnp.zeros_like(clip_s)
        for head in range(2):
            build_bias(table_ref[pl.ds(p * 2 + head, 1), :], bias_s, head)

        def block(step, _):
            i = blocks - 1 - step

            @pl.when(step == blocks - LEFT // 2)
            def _():
                for copy in prior_copies(p):
                    copy.wait_recv()
                for b in range(LEFT // 2):
                    key_tile(pk_s[p, b * BLK : (b + 1) * BLK, :], b)
                v_s[:REACH, :] = pv_s[p]

            base = pl.multiple_of(i * BLK, BLK)
            rows = pl.ds(base, BLK)
            hat, scale = normed(q_ref[rows, lanes_of(p)], ones)
            qs = stack_halves((hat * gain_q).astype(BF16) * jnp.asarray(0.125, BF16))
            gs = stack_halves(g_ref[rows, lanes_of(p)])
            peaks, penalties = [], []
            for j in range(5):
                keys = pl.ds(base + j * BLK, BLK)
                own = slice(j * BLK, (j + 1) * BLK)
                s = dot(k_s[keys, :], qs, ((1,), (1,))) + bias_s[own, :]
                s_s[own, :] = s
                dw_s[own, :] = dot(v_s[keys, :], gs, ((1,), (1,)))
                penalty = jnp.where(first & (j < 4 - i), NEG, 0.0)
                penalties.append(penalty)
                peaks.append(jnp.max(s, axis=0, keepdims=True) + penalty)
            peak = functools.reduce(jnp.maximum, peaks)
            total = jnp.zeros((1, 2 * BLK), F32)
            delta = jnp.zeros((1, 2 * BLK), F32)
            for j in range(5):
                own = slice(j * BLK, (j + 1) * BLK)
                e = jnp.exp(s_s[own, :] - (peak - penalties[j]))
                s_s[own, :] = e
                total = total + jnp.sum(e, axis=0, keepdims=True)
                delta = delta + jnp.sum(e * dw_s[own, :], axis=0, keepdims=True)
            inverse = 1.0 / total
            delta = delta * inverse
            clipped = jnp.zeros((1, 2 * BLK), F32)
            for j in range(5):
                own = slice(j * BLK, (j + 1) * BLK)
                keys = pl.ds(base + j * BLK, BLK)
                w = s_s[own, :] * inverse
                ds = w * (dw_s[own, :] - delta)
                if j < 2:
                    clipped = clipped + jnp.sum(ds, axis=0, keepdims=True)
                else:
                    acc_s[(j - 2) * BLK : (j - 1) * BLK, :] += ds
                ds_low = ds.astype(BF16)
                ds_s[own, :] = ds_low
                dk_s[slot, keys, :] += dot(ds_low, qs, ((1,), (0,)))
                dv_s[slot, keys, :] += dot(w.astype(BF16), gs, ((1,), (0,)))
            clip_s[...] += clipped
            dqt = dot(kt_s[:, pl.ds(base, BAND)], ds_s[...], ((1,), (0,)))
            dqt = jnp.concatenate([dqt[:64, :BLK], dqt[64:, BLK:]], axis=0)
            dq = dqt.T * 0.125
            gq_s[...] += jnp.sum(dq * hat, axis=0, keepdims=True)
            qg_ref[rows, lanes_of(p)] = norm_grad(dq, gain_q, hat, scale, ones).astype(BF16)
            return 0

        lax.fori_loop(0, blocks, block, 0)
        ck_s[p] = dk_s[slot, :REACH, :].astype(BF16)
        cv_s[p] = dv_s[slot, :REACH, :].astype(BF16)
        lane = lax.broadcasted_iota(jnp.int32, (1, 512), 1)
        for head in range(2):
            far = jnp.sum(clip_s[:, head * BLK : (head + 1) * BLK], axis=1, keepdims=True)
            stat_s[0, pl.ds(p * 2 + head, 1), :] = fold_bias(acc_s, head) + jnp.where(lane == 0, far, 0.0)
        for copy in cross_copies(p):
            copy.start()

        @pl.when(p > 0)
        def _():
            finish(p - 1)

        return 0

    lax.fori_loop(0, pairs, pair, 0)
    finish(pairs - 1)
    rows = stat_s.shape[1]
    stat_s[0, rows - 8 : rows - 7, 0:BLK] = gq_s[...]
    stat_s[0, rows - 8 : rows - 7, BLK : 2 * BLK] = gk_s[...]
    for r, device in enumerate(partners):
        part = slice(0, rows) if r < len(doubling(sp)) else slice(rows - 8, rows)
        copy = remote(stat_s.at[r, part], got_s.at[r, part], stat_send.at[r], stat_recv.at[r], device)
        copy.start()
        copy.wait()
        stat_s[r + 1, part] = stat_s[r, part] + got_s[r, part]
    out_ref[: rows - 8, :] = stat_s[len(doubling(sp)), : rows - 8]
    out_ref[rows - 8 :, :] = stat_s[len(partners), rows - 8 :]
    for p in range(pairs):
        for copy in prior_copies(p) + cross_copies(p):
            copy.wait_send()


def body(query_rows, key_rows, value_rows, query_gain, key_gain, position_bias, output_grad):
    heads = position_bias.shape[0]
    pairs = heads // 2
    tokens = query_rows.shape[0]
    sp, tp = lax.axis_size("sp"), lax.axis_size("tp")
    rounds = len(doubling(sp)) + len(doubling(tp))
    table = position_bias.astype(F32)
    last = jnp.broadcast_to(table[:, -1:], (heads, 129))
    table = jnp.concatenate([last, jnp.full((heads, 64), NEG, F32), table[:, :-1]], axis=1)
    gains = jnp.stack([jnp.tile(query_gain.astype(F32), 2), jnp.tile(key_gain.astype(F32), 2)])
    ext = tokens + REACH
    rows = (heads + 7) // 8 * 8 + 8
    vmem = pl.BlockSpec(memory_space=pltpu.VMEM)
    grads = jax.ShapeDtypeStruct((tokens, heads * 64), BF16)
    sems = pltpu.SemaphoreType.DMA
    query_grad, key_grad, value_grad, stats = pl.pallas_call(
        functools.partial(kernel, sp, tp),
        in_specs=[vmem] * 6,
        out_specs=[vmem] * 4,
        out_shape=[grads, grads, grads, jax.ShapeDtypeStruct((rows, 512), F32)],
        scratch_shapes=[
            pltpu.VMEM((ext, BLK), BF16), pltpu.VMEM((BLK, ext), BF16), pltpu.VMEM((ext, BLK), BF16),
            pltpu.VMEM((BAND, 2 * BLK), F32), pltpu.VMEM((3 * BLK, 2 * BLK), F32),
            pltpu.VMEM((BAND, 2 * BLK), F32), pltpu.VMEM((BAND, 2 * BLK), F32),
            pltpu.VMEM((BAND, 2 * BLK), BF16),
            pltpu.VMEM((2, ext, BLK), F32), pltpu.VMEM((2, ext, BLK), F32),
            pltpu.VMEM((1, 2 * BLK), F32), pltpu.VMEM((1, BLK), F32), pltpu.VMEM((1, BLK), F32),
        ]
        + [pltpu.VMEM((pairs, REACH, BLK), BF16)] * 6
        + [
            pltpu.VMEM((rounds + 1, rows, 512), F32), pltpu.VMEM((rounds, rows, 512), F32),
            sems((2, pairs)), sems((2, pairs)), sems((2, pairs)), sems((2, pairs)),
            sems((rounds,)), sems((rounds,)),
        ],
        compiler_params=pltpu.CompilerParams(collective_id=0, has_side_effects=True, vmem_limit_bytes=48 << 20),
        name="attend",
    )(query_rows, key_rows, value_rows, output_grad, gains, table)
    fold = stats[:heads]
    bias_grad = jnp.concatenate([fold[:, 193:], jnp.sum(fold[:, :129], axis=1, keepdims=True)], axis=1)
    gain_row = stats[rows - 8]
    query_gain_grad = gain_row[:64] + gain_row[64:128]
    key_gain_grad = gain_row[128:192] + gain_row[192:256]
    return (query_grad, key_grad, value_grad, bias_grad, query_gain_grad, key_gain_grad)


def solution(mesh):
    placed = (P("sp", "tp"), P("sp", "tp"), P("sp", "tp"), P(), P(), P("tp", None), P("sp", "tp"))
    return jax.shard_map(
        body,
        mesh=mesh,
        in_specs=placed,
        out_specs=(P("sp", "tp"), P("sp", "tp"), P("sp", "tp"), P("tp", None), P(), P()),
        check_vma=False,
    )
```

time: 195 us -> 93.6 us (0.48)
  blocking collectives: 117 us -> 0 us
  Pallas kernels: 56.1 us -> 81.6 us
  starting transfers between devices: 9.56 us -> 0 us
    psum x2 -> x0, blocking collectives: 117 us -> none  [the longest x1 80.2 us: body(): bias_grad = lax.psum(bias_part, 'sp')]
    pallas_call x2 -> x1, Pallas kernels: 56.1 us -> 81.6 us  [body(): pl.pallas_call(functools.partial(kernel, sp, tp), in_specs=[vmem] * 6, ou...]
    ppermute x4 -> x0, starting transfers between devices: 9.56 us -> none  [passed_along(): return lax.ppermute(block, axis, route)]
    unnamed x16 -> x15, local copies, waits for them, and re-layouts: 2.9 us -> 8.03 us
    pallas_call x3 -> x0, other arithmetic: 2.1 us -> none  [the longest x2 1.41 us: body(): pl.pallas_call(main_kernel, grid=(pairs,), in_specs=[full, full, full, fu...]
  transfers between devices with their start and end apart: 4 -> 0, of which waited for: 0 -> 0; matrix products, arithmetic and copies ran while one was open for 2% -> 0% of each run, Pallas kernels for 0% -> 0%
where the time goes in v2:
time: 93.6 us; the launch traced here: 93.2 us
  Pallas kernels  81.6 us (87%)
  local copies, waits for them, and re-layouts  8.71 us (9%)
  other arithmetic  2.19 us (2%)
    pallas_call x1, Pallas kernels, body(): pl.pallas_call(functools.partial(kernel, sp, tp), in_specs=[vmem] * 6, ou...  81.6 us
    unnamed x15, local copies, waits for them, and re-layouts  8.03 us

profile of v2, /device:TPU:0, one launch (start us, length us, event | category | flops | bytes accessed | tf_op | source)
XLA Modules:
  0.0 93.2 jit_solution(16986984059366647823)
XLA Ops:
  0.6 0.7 convert_element_type.11
  1.3 0.0 copy-start.3
  1.3 0.2 slice_reduce_fusion.1
  1.5 0.1 broadcast_in_dim.14
  1.6 0.4 copy-done.3
  2.1 0.1 pad.3.clone
  2.1 0.0 copy-start.4
  2.1 0.1 pad_maximum_fusion.table_ref
  2.2 0.6 copy-done.4
  2.8 0.0 copy-start.5
  2.8 0.1 stack_tile.6
  2.9 0.6 copy-done.5
  3.5 0.1 stack_tile.7
  3.5 0.0 copy-start
  3.6 1.2 %copy-done = bf16[640,768]{1,0:T(8,128)(2,1)S(1)} copy-done((bf16[640,768]{1,0:T(8,128)(2,1)S(1)}, bf16[640,768]{1,0:T(8,128)(2,1)}, u32[]{:S(2)}) %copy-start) | copy-done | bytes 983064
  4.8 0.0 copy-start.1
  4.8 1.2 %copy-done.1 = bf16[640,768]{1,0:T(8,128)(2,1)S(1)} copy-done((bf16[640,768]{1,0:T(8,128)(2,1)S(1)}, bf16[640,768]{1,0:T(8,128)(2,1)}, u32[]{:S(2)}) %copy-start.1) | copy-done | bytes 983064
  6.0 0.0 copy-start.2
  6.0 1.2 %copy-done.2 = bf16[640,768]{1,0:T(8,128)(2,1)S(1)} copy-done((bf16[640,768]{1,0:T(8,128)(2,1)S(1)}, bf16[640,768]{1,0:T(8,128)(2,1)}, u32[]{:S(2)}) %copy-start.2) | copy-done | bytes 983064
  7.2 81.6 %attend.1 = (bf16[640,768]{1,0:T(8,128)(2,1)S(1)}, bf16[640,768]{1,0:T(8,128)(2,1)S(1)}, bf16[640,768]{1,0:T(8,128)(2,1)S(1)}, f32[24,512]{1,0:T(8,128)S(1)}) custom-call(bf16[640,768]{1,0:T(8,128)(2,1)S(1)} %copy-done, bf16[640,768]{1,0:T(8,128)(2,1)S(1)} %copy-done.1, bf16[640,768]{1,0:T(8,128)(2,1)S(1)} %copy-done.2, bf16[640,768]{1,0:T(8,128)(2,1)} %g_ref.1, ...), custom_call_target="tpu_custom_call" | custom-call | tf_op jit(solution)/shard_map/attend/pallas_call | solution.py:297
  88.8 0.1 slice.38
  88.9 0.1 slice_reduce_fusion
  89.0 0.1 copy.14
  89.1 0.7 pad_maximum_fusion.1
  89.8 0.6 add_bitcast_fusion
  90.4 0.9 %copy.18 = bf16[640,768]{1,0:T(8,128)(2,1)} copy(bf16[640,768]{1,0:T(8,128)(2,1)S(1)} %get-tuple-element.22) | data formatting | bytes 1966080
  91.3 0.9 %copy.19 = bf16[640,768]{1,0:T(8,128)(2,1)} copy(bf16[640,768]{1,0:T(8,128)(2,1)S(1)} %get-tuple-element.23) | data formatting | bytes 1966080
  92.3 0.9 %copy.20 = bf16[640,768]{1,0:T(8,128)(2,1)} copy(bf16[640,768]{1,0:T(8,128)(2,1)S(1)} %get-tuple-element.24) | data formatting | bytes 1966080
  (5 shorter events, 0.0 us)
Async XLA Ops:
  1.3 0.7 copy-start.3
  2.1 0.7 copy-start.4
  2.8 0.7 copy-start.5
  3.5 1.2 %copy-start = (bf16[640,768]{1,0:T(8,128)(2,1)S(1)}, bf16[640,768]{1,0:T(8,128)(2,1)}, u32[]{:S(2)}) copy-start(bf16[640,768]{1,0:T(8,128)(2,1)} %q_ref.1) | copy-start | bytes 2949124
  4.8 1.2 %copy-start.1 = (bf16[640,768]{1,0:T(8,128)(2,1)S(1)}, bf16[640,768]{1,0:T(8,128)(2,1)}, u32[]{:S(2)}) copy-start(bf16[640,768]{1,0:T(8,128)(2,1)} %k_ref.1) | copy-start | bytes 2949124
  6.0 1.2 %copy-start.2 = (bf16[640,768]{1,0:T(8,128)(2,1)S(1)}, bf16[640,768]{1,0:T(8,128)(2,1)}, u32[]{:S(2)}) copy-start(bf16[640,768]{1,0:T(8,128)(2,1)} %v_ref.1) | copy-start | bytes 2949124

commit v3 on v2

--- a/solution.py
+++ b/solution.py
@@ -87,20 +87,27 @@
     return wide[0:1]
 
 
-def flip(index, distance):
-    return index + distance * (1 - 2 * ((index // distance) % 2))
-
-
-def doubling(size):
-    return [1 << r for r in range(size.bit_length() - 1)]
+def rounds_of(axis, size):
+    rounds, stride = [], 1
+    while stride < size:
+        radix = 4 if size // stride % 4 == 0 else 2
+        rounds.append((axis, stride, radix))
+        stride *= radix
+    return rounds
+
+
+def peer(index, stride, radix, step):
+    digit = (index // stride) % radix
+    return index + stride * ((digit + step) % radix - digit)
 
 
 def kernel(
-    sp, tp, q_ref, k_ref, v_ref, g_ref, gains_ref, table_ref,
+    sp, tp, q_hbm, k_hbm, v_hbm, g_hbm, gains_ref, table_ref,
     qg_ref, kg_ref, vg_ref, out_ref,
-    k_s, kt_s, v_s, bias_s, acc_s, s_s, dw_s, ds_s, dk_s, dv_s, clip_s, gq_s, gk_s,
+    q_ref, k_ref, v_ref, g_ref,
+    k_s, kt_s, v_s, bias_s, acc_s, s_s, dw_s, ds_s, w_s, qs_s, gs_s, hat_s, scale_s, dk_s, dv_s, clip_s, gq_s, gk_s,
     pk_s, pv_s, ck_s, cv_s, bk_s, bv_s, stat_s, got_s,
-    prior_send, prior_recv, cross_send, cross_recv, stat_send, stat_recv,
+    prior_send, prior_recv, cross_send, cross_recv, stat_send, stat_recv, load_sem,
 ):
     tokens = q_ref.shape[0]
     blocks = tokens // BLK
@@ -108,11 +115,29 @@
     me = lax.axis_index("sp")
     me_tp = lax.axis_index("tp")
     right, left = lax.rem(me + 1, sp), lax.rem(me + sp - 1, sp)
-    partners = [{"sp": flip(me, d)} for d in doubling(sp)] + [{"tp": flip(me_tp, d)} for d in doubling(tp)]
+    rounds = rounds_of("sp", sp) + rounds_of("tp", tp)
+    peers = [
+        [{axis: peer(me if axis == "sp" else me_tp, stride, radix, k)} for k in range(1, radix)]
+        for axis, stride, radix in rounds
+    ]
     first = me == 0
 
+    def lanes_of(p):
+        return pl.ds(pl.multiple_of(p * BLK, BLK), BLK)
+
+    def loads(p):
+        moves = ((k_hbm, k_ref), (q_hbm, q_ref), (v_hbm, v_ref), (g_hbm, g_ref))
+        return [
+            pltpu.make_async_copy(src.at[:, lanes_of(p)], dst.at[:, lanes_of(p)], load_sem.at[n, p])
+            for n, (src, dst) in enumerate(moves)
+        ]
+
+    for p in range(pairs):
+        for copy in loads(p):
+            copy.start()
+
     barrier = pltpu.get_barrier_semaphore()
-    greeted = [{"sp": right}, {"sp": left}] + partners
+    greeted = [{"sp": right}, {"sp": left}] + [device for group in peers for device in group]
     for device in greeted:
         pl.semaphore_signal(barrier, inc=1, device_id=device, device_id_type=pl.DeviceIdType.MESH)
     pl.semaphore_wait(barrier, len(greeted))
@@ -123,14 +148,11 @@
             device_id=device, device_id_type=pl.DeviceIdType.MESH,
         )
 
-    def lanes_of(p):
-        return pl.ds(pl.multiple_of(p * BLK, BLK), BLK)
-
     def prior_copies(p):
         rows = slice(tokens - REACH, tokens)
         return (
-            remote(k_ref.at[rows, lanes_of(p)], pk_s.at[p], prior_send.at[0, p], prior_recv.at[0, p], {"sp": right}),
-            remote(v_ref.at[rows, lanes_of(p)], pv_s.at[p], prior_send.at[1, p], prior_recv.at[1, p], {"sp": right}),
+            remote(k_hbm.at[rows, lanes_of(p)], pk_s.at[p], prior_send.at[0, p], prior_recv.at[0, p], {"sp": right}),
+            remote(v_hbm.at[rows, lanes_of(p)], pv_s.at[p], prior_send.at[1, p], prior_recv.at[1, p], {"sp": right}),
         )
 
     def cross_copies(p):
@@ -176,76 +198,91 @@
 
     def pair(p, _):
         slot = lax.rem(p, 2)
-        for b in range(blocks):
-            key_tile(k_ref[b * BLK : (b + 1) * BLK, lanes_of(p)], b + LEFT // 2)
-        v_s[REACH:, :] = v_ref[:, lanes_of(p)]
+        for head in range(2):
+            build_bias(table_ref[pl.ds(p * 2 + head, 1), :], bias_s, head)
         dk_s[slot] = jnp.zeros(dk_s.shape[1:], F32)
         dv_s[slot] = jnp.zeros(dv_s.shape[1:], F32)
         acc_s[...] = jnp.zeros_like(acc_s)
         clip_s[...] = jnp.zeros_like(clip_s)
-        for head in range(2):
-            build_bias(table_ref[pl.ds(p * 2 + head, 1), :], bias_s, head)
-
-        def block(step, _):
-            i = blocks - 1 - step
-
-            @pl.when(step == blocks - LEFT // 2)
-            def _():
-                for copy in prior_copies(p):
-                    copy.wait_recv()
-                for b in range(LEFT // 2):
-                    key_tile(pk_s[p, b * BLK : (b + 1) * BLK, :], b)
-                v_s[:REACH, :] = pv_s[p]
-
-            base = pl.multiple_of(i * BLK, BLK)
-            rows = pl.ds(base, BLK)
+        for copy in loads(p):
+            copy.wait()
+        for b in range(blocks):
+            rows = slice(b * BLK, (b + 1) * BLK)
+            key_tile(k_ref[rows, lanes_of(p)], b + LEFT // 2)
             hat, scale = normed(q_ref[rows, lanes_of(p)], ones)
-            qs = stack_halves((hat * gain_q).astype(BF16) * jnp.asarray(0.125, BF16))
-            gs = stack_halves(g_ref[rows, lanes_of(p)])
-            peaks, penalties = [], []
-            for j in range(5):
-                keys = pl.ds(base + j * BLK, BLK)
-                own = slice(j * BLK, (j + 1) * BLK)
-                s = dot(k_s[keys, :], qs, ((1,), (1,))) + bias_s[own, :]
-                s_s[own, :] = s
-                dw_s[own, :] = dot(v_s[keys, :], gs, ((1,), (1,)))
-                penalty = jnp.where(first & (j < 4 - i), NEG, 0.0)
-                penalties.append(penalty)
-                peaks.append(jnp.max(s, axis=0, keepdims=True) + penalty)
-            peak = functools.reduce(jnp.maximum, peaks)
-            total = jnp.zeros((1, 2 * BLK), F32)
-            delta = jnp.zeros((1, 2 * BLK), F32)
-            for j in range(5):
-                own = slice(j * BLK, (j + 1) * BLK)
-                e = jnp.exp(s_s[own, :] - (peak - penalties[j]))
-                s_s[own, :] = e
-                total = total + jnp.sum(e, axis=0, keepdims=True)
-                delta = delta + jnp.sum(e * dw_s[own, :], axis=0, keepdims=True)
-            inverse = 1.0 / total
-            delta = delta * inverse
-            clipped = jnp.zeros((1, 2 * BLK), F32)
-            for j in range(5):
-                own = slice(j * BLK, (j + 1) * BLK)
-                keys = pl.ds(base + j * BLK, BLK)
-                w = s_s[own, :] * inverse
-                ds = w * (dw_s[own, :] - delta)
-                if j < 2:
-                    clipped = clipped + jnp.sum(ds, axis=0, keepdims=True)
-                else:
-                    acc_s[(j - 2) * BLK : (j - 1) * BLK, :] += ds
-                ds_low = ds.astype(BF16)
-                ds_s[own, :] = ds_low
-                dk_s[slot, keys, :] += dot(ds_low, qs, ((1,), (0,)))
-                dv_s[slot, keys, :] += dot(w.astype(BF16), gs, ((1,), (0,)))
-            clip_s[...] += clipped
-            dqt = dot(kt_s[:, pl.ds(base, BAND)], ds_s[...], ((1,), (0,)))
+            hat_s[rows, :] = hat
+            scale_s[rows, :] = scale
+            qs_s[b] = stack_halves((hat * gain_q).astype(BF16) * jnp.asarray(0.125, BF16))
+            gs_s[b] = stack_halves(g_ref[rows, lanes_of(p)])
+        v_s[REACH:, :] = v_ref[:, lanes_of(p)]
+        for copy in prior_copies(p):
+            copy.wait_recv()
+        for b in range(LEFT // 2):
+            key_tile(pk_s[p, b * BLK : (b + 1) * BLK, :], b)
+        v_s[:REACH, :] = pv_s[p]
+
+        def tile(j):
+            return slice(j * BLK, (j + 1) * BLK)
+
+        def score(i, j, peaks):
+            keys = tile(i + j)
+            s = dot(k_s[keys, :], qs_s[i], ((1,), (1,))) + bias_s[tile(j), :]
+            s_s[i % 2, tile(j), :] = s
+            dw_s[i % 2, tile(j), :] = dot(v_s[keys, :], gs_s[i], ((1,), (1,)))
+            top = jnp.max(s, axis=0, keepdims=True)
+            peaks.append(top + penalty if j < LEFT // 2 - i else top)
+
+        def product(i, j):
+            keys = tile(i + j)
+            dk_s[slot, keys, :] += dot(ds_s[i % 2, tile(j), :], qs_s[i], ((1,), (0,)))
+            dv_s[slot, keys, :] += dot(w_s[i % 2, tile(j), :], gs_s[i], ((1,), (0,)))
+
+        def query_side(i):
+            rows = tile(i)
+            dqt = dot(kt_s[:, i * BLK : i * BLK + BAND], ds_s[i % 2], ((1,), (0,)))
             dqt = jnp.concatenate([dqt[:64, :BLK], dqt[64:, BLK:]], axis=0)
             dq = dqt.T * 0.125
+            hat = hat_s[rows, :]
             gq_s[...] += jnp.sum(dq * hat, axis=0, keepdims=True)
-            qg_ref[rows, lanes_of(p)] = norm_grad(dq, gain_q, hat, scale, ones).astype(BF16)
-            return 0
-
-        lax.fori_loop(0, blocks, block, 0)
+            qg_ref[rows, lanes_of(p)] = norm_grad(dq, gain_q, hat, scale_s[rows, :], ones).astype(BF16)
+
+        penalty = jnp.where(first, NEG, 0.0)
+        peaks = {}
+        for step in range(blocks + 2):
+            ahead, here, behind = step, step - 1, step - 2
+            peaks[ahead] = []
+            if 0 <= here < blocks:
+                peak = functools.reduce(jnp.maximum, peaks[here])
+                total = jnp.zeros((1, 2 * BLK), F32)
+                delta = jnp.zeros((1, 2 * BLK), F32)
+                clipped = jnp.zeros((1, 2 * BLK), F32)
+            for j in range(5):
+                if ahead < blocks:
+                    score(ahead, j, peaks[ahead])
+                if 0 <= here < blocks:
+                    e = jnp.exp(s_s[here % 2, tile(j), :] - (peak - penalty if j < LEFT // 2 - here else peak))
+                    s_s[here % 2, tile(j), :] = e
+                    total = total + jnp.sum(e, axis=0, keepdims=True)
+                    delta = delta + jnp.sum(e * dw_s[here % 2, tile(j), :], axis=0, keepdims=True)
+            if 0 <= here < blocks:
+                inverse = 1.0 / total
+                delta = delta * inverse
+            if behind >= 0:
+                query_side(behind)
+            for j in range(5):
+                if behind >= 0:
+                    product(behind, j)
+                if 0 <= here < blocks:
+                    w = s_s[here % 2, tile(j), :] * inverse
+                    ds = w * (dw_s[here % 2, tile(j), :] - delta)
+                    if j < 2:
+                        clipped = clipped + jnp.sum(ds, axis=0, keepdims=True)
+                    else:
+                        acc_s[tile(j - 2), :] += ds
+                    ds_s[here % 2, tile(j), :] = ds.astype(BF16)
+                    w_s[here % 2, tile(j), :] = w.astype(BF16)
+            if 0 <= here < blocks:
+                clip_s[...] += clipped
         ck_s[p] = dk_s[slot, :REACH, :].astype(BF16)
         cv_s[p] = dv_s[slot, :REACH, :].astype(BF16)
         lane = lax.broadcasted_iota(jnp.int32, (1, 512), 1)
@@ -266,14 +303,23 @@
     rows = stat_s.shape[1]
     stat_s[0, rows - 8 : rows - 7, 0:BLK] = gq_s[...]
     stat_s[0, rows - 8 : rows - 7, BLK : 2 * BLK] = gk_s[...]
-    for r, device in enumerate(partners):
-        part = slice(0, rows) if r < len(doubling(sp)) else slice(rows - 8, rows)
-        copy = remote(stat_s.at[r, part], got_s.at[r, part], stat_send.at[r], stat_recv.at[r], device)
-        copy.start()
-        copy.wait()
-        stat_s[r + 1, part] = stat_s[r, part] + got_s[r, part]
-    out_ref[: rows - 8, :] = stat_s[len(doubling(sp)), : rows - 8]
-    out_ref[rows - 8 :, :] = stat_s[len(partners), rows - 8 :]
+    summed = len(rounds_of("sp", sp))
+    for r, group in enumerate(peers):
+        part = slice(0, rows) if r < summed else slice(rows - 8, rows)
+        copies = [
+            remote(stat_s.at[r, part], got_s.at[r, k, part], stat_send.at[r, k], stat_recv.at[r, k], device)
+            for k, device in enumerate(group)
+        ]
+        for copy in copies:
+            copy.start()
+        for copy in copies:
+            copy.wait()
+        if len(group) == 3:
+            stat_s[r + 1, part] = (stat_s[r, part] + got_s[r, 1, part]) + (got_s[r, 0, part] + got_s[r, 2, part])
+        else:
+            stat_s[r + 1, part] = stat_s[r, part] + got_s[r, 0, part]
+    out_ref[: rows - 8, :] = stat_s[summed, : rows - 8]
+    out_ref[rows - 8 :, :] = stat_s[len(peers), rows - 8 :]
     for p in range(pairs):
         for copy in prior_copies(p) + cross_copies(p):
             copy.wait_send()
@@ -284,7 +330,7 @@
     pairs = heads // 2
     tokens = query_rows.shape[0]
     sp, tp = lax.axis_size("sp"), lax.axis_size("tp")
-    rounds = len(doubling(sp)) + len(doubling(tp))
+    rounds = len(rounds_of("sp", sp) + rounds_of("tp", tp))
     table = position_bias.astype(F32)
     last = jnp.broadcast_to(table[:, -1:], (heads, 129))
     table = jnp.concatenate([last, jnp.full((heads, 64), NEG, F32), table[:, :-1]], axis=1)
@@ -296,22 +342,25 @@
     sems = pltpu.SemaphoreType.DMA
     query_grad, key_grad, value_grad, stats = pl.pallas_call(
         functools.partial(kernel, sp, tp),
-        in_specs=[vmem] * 6,
+        in_specs=[pl.BlockSpec(memory_space=pltpu.HBM)] * 4 + [vmem] * 2,
         out_specs=[vmem] * 4,
         out_shape=[grads, grads, grads, jax.ShapeDtypeStruct((rows, 512), F32)],
-        scratch_shapes=[
+        scratch_shapes=[pltpu.VMEM((tokens, heads * 64), BF16)] * 4
+        + [
             pltpu.VMEM((ext, BLK), BF16), pltpu.VMEM((BLK, ext), BF16), pltpu.VMEM((ext, BLK), BF16),
             pltpu.VMEM((BAND, 2 * BLK), F32), pltpu.VMEM((3 * BLK, 2 * BLK), F32),
-            pltpu.VMEM((BAND, 2 * BLK), F32), pltpu.VMEM((BAND, 2 * BLK), F32),
-            pltpu.VMEM((BAND, 2 * BLK), BF16),
+            pltpu.VMEM((2, BAND, 2 * BLK), F32), pltpu.VMEM((2, BAND, 2 * BLK), F32),
+            pltpu.VMEM((2, BAND, 2 * BLK), BF16), pltpu.VMEM((2, BAND, 2 * BLK), BF16),
+            pltpu.VMEM((tokens // BLK, 2 * BLK, BLK), BF16), pltpu.VMEM((tokens // BLK, 2 * BLK, BLK), BF16),
+            pltpu.VMEM((tokens, BLK), F32), pltpu.VMEM((tokens, BLK), F32),
             pltpu.VMEM((2, ext, BLK), F32), pltpu.VMEM((2, ext, BLK), F32),
             pltpu.VMEM((1, 2 * BLK), F32), pltpu.VMEM((1, BLK), F32), pltpu.VMEM((1, BLK), F32),
         ]
         + [pltpu.VMEM((pairs, REACH, BLK), BF16)] * 6
         + [
-            pltpu.VMEM((rounds + 1, rows, 512), F32), pltpu.VMEM((rounds, rows, 512), F32),
+            pltpu.VMEM((rounds + 1, rows, 512), F32), pltpu.VMEM((rounds, 3, rows, 512), F32),
             sems((2, pairs)), sems((2, pairs)), sems((2, pairs)), sems((2, pairs)),
-            sems((rounds,)), sems((rounds,)),
+            sems((rounds, 3)), sems((rounds, 3)), sems((4, pairs)),
         ],
         compiler_params=pltpu.CompilerParams(collective_id=0, has_side_effects=True, vmem_limit_bytes=48 << 20),
         name="attend",

time: 93.6 us -> 74.4 us (0.79)
  Pallas kernels: 81.6 us -> 62.5 us
    pallas_call x1, Pallas kernels: 81.6 us -> 62.5 us  [body(): pl.pallas_call(functools.partial(kernel, sp, tp), in_specs=[pl.BlockSpec(...]
where the time goes in v3:
time: 74.4 us; the launch traced here: 74 us
  Pallas kernels  62.5 us (84%)
  local copies, waits for them, and re-layouts  8.71 us (12%)
  other arithmetic  2.19 us (3%)
    pallas_call x1, Pallas kernels, body(): pl.pallas_call(functools.partial(kernel, sp, tp), in_specs=[pl.BlockSpec(...  62.5 us
    unnamed x15, local copies, waits for them, and re-layouts  8.03 us

profile of v3, /device:TPU:0, one launch (start us, length us, event | category | flops | bytes accessed | tf_op | source)
XLA Modules:
  0.0 74.0 jit_solution(14890223110260275351)
XLA Ops:
  0.6 0.7 convert_element_type.11
  1.3 0.0 copy-start.3
  1.3 0.2 slice_reduce_fusion.1
  1.5 0.1 broadcast_in_dim.14
  1.6 0.4 copy-done.3
  2.1 0.1 pad.3.clone
  2.1 0.0 copy-start.4
  2.1 0.1 pad_maximum_fusion.table_ref
  2.2 0.6 copy-done.4
  2.8 0.0 copy-start.5
  2.8 0.1 stack_tile.6
  2.9 0.6 copy-done.5
  3.5 0.1 stack_tile.7
  3.5 0.0 copy-start
  3.6 1.2 %copy-done = bf16[640,768]{1,0:T(8,128)(2,1)S(1)} copy-done((bf16[640,768]{1,0:T(8,128)(2,1)S(1)}, bf16[640,768]{1,0:T(8,128)(2,1)}, u32[]{:S(2)}) %copy-start) | copy-done | bytes 983064
  4.8 0.0 copy-start.1
  4.8 1.2 %copy-done.1 = bf16[640,768]{1,0:T(8,128)(2,1)S(1)} copy-done((bf16[640,768]{1,0:T(8,128)(2,1)S(1)}, bf16[640,768]{1,0:T(8,128)(2,1)}, u32[]{:S(2)}) %copy-start.1) | copy-done | bytes 983064
  6.0 0.0 copy-start.2
  6.0 1.2 %copy-done.2 = bf16[640,768]{1,0:T(8,128)(2,1)S(1)} copy-done((bf16[640,768]{1,0:T(8,128)(2,1)S(1)}, bf16[640,768]{1,0:T(8,128)(2,1)}, u32[]{:S(2)}) %copy-start.2) | copy-done | bytes 983064
  7.2 62.5 %attend.1 = (bf16[640,768]{1,0:T(8,128)(2,1)S(1)}, bf16[640,768]{1,0:T(8,128)(2,1)S(1)}, bf16[640,768]{1,0:T(8,128)(2,1)S(1)}, f32[24,512]{1,0:T(8,128)S(1)}) custom-call(bf16[640,768]{1,0:T(8,128)(2,1)S(1)} %copy-done, bf16[640,768]{1,0:T(8,128)(2,1)S(1)} %copy-done.1, bf16[640,768]{1,0:T(8,128)(2,1)S(1)} %copy-done.2, bf16[640,768]{1,0:T(8,128)(2,1)} %g_hbm.1, ...), custom_call_target="tpu_custom_call" | custom-call | tf_op jit(solution)/shard_map/attend/pallas_call | solution.py:343
  69.6 0.1 slice.38
  69.7 0.1 slice_reduce_fusion
  69.8 0.1 copy.14
  69.9 0.7 pad_maximum_fusion.1
  70.6 0.6 add_bitcast_fusion
  71.2 0.9 %copy.18 = bf16[640,768]{1,0:T(8,128)(2,1)} copy(bf16[640,768]{1,0:T(8,128)(2,1)S(1)} %get-tuple-element.22) | data formatting | bytes 1966080
  72.1 0.9 %copy.19 = bf16[640,768]{1,0:T(8,128)(2,1)} copy(bf16[640,768]{1,0:T(8,128)(2,1)S(1)} %get-tuple-element.23) | data formatting | bytes 1966080
  73.1 0.9 %copy.20 = bf16[640,768]{1,0:T(8,128)(2,1)} copy(bf16[640,768]{1,0:T(8,128)(2,1)S(1)} %get-tuple-element.24) | data formatting | bytes 1966080
  (5 shorter events, 0.0 us)
Async XLA Ops:
  1.3 0.7 copy-start.3
  2.1 0.7 copy-start.4
  2.8 0.7 copy-start.5
  3.5 1.2 %copy-start = (bf16[640,768]{1,0:T(8,128)(2,1)S(1)}, bf16[640,768]{1,0:T(8,128)(2,1)}, u32[]{:S(2)}) copy-start(bf16[640,768]{1,0:T(8,128)(2,1)} %q_hbm.1) | copy-start | bytes 2949124
  4.8 1.2 %copy-start.1 = (bf16[640,768]{1,0:T(8,128)(2,1)S(1)}, bf16[640,768]{1,0:T(8,128)(2,1)}, u32[]{:S(2)}) copy-start(bf16[640,768]{1,0:T(8,128)(2,1)} %k_hbm.1) | copy-start | bytes 2949124
  6.0 1.2 %copy-start.2 = (bf16[640,768]{1,0:T(8,128)(2,1)S(1)}, bf16[640,768]{1,0:T(8,128)(2,1)}, u32[]{:S(2)}) copy-start(bf16[640,768]{1,0:T(8,128)(2,1)} %v_hbm.1) | copy-start | bytes 2949124

commit v4 on v3

--- a/solution.py
+++ b/solution.py
@@ -362,7 +362,7 @@
             sems((2, pairs)), sems((2, pairs)), sems((2, pairs)), sems((2, pairs)),
             sems((rounds, 3)), sems((rounds, 3)), sems((4, pairs)),
         ],
-        compiler_params=pltpu.CompilerParams(collective_id=0, has_side_effects=True, vmem_limit_bytes=48 << 20),
+        compiler_params=pltpu.CompilerParams(collective_id=0, has_side_effects=True, vmem_limit_bytes=67_043_328),
         name="attend",
     )(query_rows, key_rows, value_rows, output_grad, gains, table)
     fold = stats[:heads]

time: 74.4 us -> 77.8 us (1.046)
  other arithmetic: 2.19 us -> 4.84 us
  Pallas kernels: 62.5 us -> 64.6 us
  local copies, waits for them, and re-layouts: 8.71 us -> 7.24 us
    unnamed x15 -> x13, local copies, waits for them, and re-layouts: 8.03 us -> 5.82 us
    pallas_call x1, Pallas kernels: 62.5 us -> 64.6 us  [body(): pl.pallas_call(functools.partial(kernel, sp, tp), in_specs=[pl.BlockSpec(...]
where the time goes in v4:
time: 77.8 us; the launch traced here: 77.3 us
  Pallas kernels  64.6 us (83%)
  local copies, waits for them, and re-layouts  7.24 us (9%)
  other arithmetic  4.84 us (6%)
    pallas_call x1, Pallas kernels, body(): pl.pallas_call(functools.partial(kernel, sp, tp), in_specs=[pl.BlockSpec(...  64.6 us
    unnamed x13, local copies, waits for them, and re-layouts  5.82 us

profile of v4, /device:TPU:0, one launch (start us, length us, event | category | flops | bytes accessed | tf_op | source)
XLA Modules:
  0.0 77.3 jit_solution(1093609594998288579)
XLA Ops:
  0.6 0.7 convert_element_type.11
  1.3 0.0 copy-start.2
  1.3 0.2 slice_reduce_fusion.1
  1.5 0.1 broadcast_in_dim.14
  1.6 0.4 copy-done.2
  2.1 0.1 pad.3.clone
  2.1 0.0 copy-start.3
  2.1 0.7 pad_maximum_fusion.table_ref
  2.8 0.0 copy-done.3
  2.8 0.0 copy-start.4
  2.8 0.1 stack_tile.6
  2.9 0.6 copy-done.4
  3.5 0.1 stack_tile.7
  3.6 0.6 pad_maximum_fusion.2.gains_ref
  4.2 64.6 %attend.1 = (bf16[640,768]{1,0:T(8,128)(2,1)}, bf16[640,768]{1,0:T(8,128)(2,1)}, bf16[640,768]{1,0:T(8,128)(2,1)}, f32[24,512]{1,0:T(8,128)}) custom-call(bf16[640,768]{1,0:T(8,128)(2,1)} %q_hbm.1, bf16[640,768]{1,0:T(8,128)(2,1)} %k_hbm.1, bf16[640,768]{1,0:T(8,128)(2,1)} %v_hbm.1, bf16[640,768]{1,0:T(8,128)(2,1)} %g_hbm.1, ...), custom_call_target="tpu_custom_call" | custom-call | tf_op jit(solution)/shard_map/attend/pallas_call | solution.py:343
  68.7 0.8 %slice.38 = f32[12,319]{1,0:T(8,128)S(1)} slice(f32[24,512]{1,0:T(8,128)} %get-tuple-element.13), slice={[0:12], [193:512]} | slice | bytes 30624 | tf_op jit(solution)/shard_map/slice | solution.py:369
  69.5 0.8 %slice_reduce_fusion = f32[12]{0:T(128)S(1)} fusion(f32[24,512]{1,0:T(8,128)} %get-tuple-element.13), kind=kLoop, calls=%fused_computation.2 | loop fusion | flops 1536 | bytes 6240 | tf_op jit(solution)/shard_map/reduce_sum | solution.py:369
  70.4 0.1 copy.14
  70.5 0.7 pad_maximum_fusion.1
  71.2 1.3 %add_bitcast_fusion = (f32[64]{0:T(128)}, f32[64]{0:T(128)}) fusion(f32[24,512]{1,0:T(8,128)} %get-tuple-element.13), kind=kLoop, calls=%fused_computation.5 | loop fusion | flops 128 | bytes 1536 | tf_op jit(solution)/shard_map/add | solution.py:372
  72.5 0.0 copy-start.1
  72.5 2.3 %copy.18 = bf16[640,768]{1,0:T(8,128)(2,1)} copy(bf16[640,768]{1,0:T(8,128)(2,1)} %get-tuple-element.22) | data formatting | bytes 1966080
  74.8 0.0 copy-done.1
  74.8 0.0 copy-start
  74.8 0.9 %copy.19 = bf16[640,768]{1,0:T(8,128)(2,1)} copy(bf16[640,768]{1,0:T(8,128)(2,1)S(1)} %copy-done.1) | data formatting | bytes 1966080
  75.7 0.6 copy-done
  76.3 0.9 %copy.20 = bf16[640,768]{1,0:T(8,128)(2,1)} copy(bf16[640,768]{1,0:T(8,128)(2,1)S(1)} %copy-done) | data formatting | bytes 1966080
  (4 shorter events, 0.0 us)
Async XLA Ops:
  1.3 0.7 copy-start.2
  2.1 0.7 copy-start.3
  2.8 0.7 copy-start.4
  72.5 2.3 %copy-start.1 = (bf16[640,768]{1,0:T(8,128)(2,1)S(1)}, bf16[640,768]{1,0:T(8,128)(2,1)}, u32[]{:S(2)}) copy-start(bf16[640,768]{1,0:T(8,128)(2,1)} %get-tuple-element.23) | copy-start | bytes 2949124
  74.8 1.6 %copy-start = (bf16[640,768]{1,0:T(8,128)(2,1)S(1)}, bf16[640,768]{1,0:T(8,128)(2,1)}, u32[]{:S(2)}) copy-start(bf16[640,768]{1,0:T(8,128)(2,1)} %get-tuple-element.24) | copy-start | bytes 2949124
